TPU v7x, 128 devices: a whole 4x4x4 slice. The times are simulated.
128 devices in a mesh: ra: 16 (over z, x), cb: 4 (over y), dp: 2 (over core).
Axes of the slice: x: 4, y: 4, z: 4, core: 2. Of those that a mesh axis runs over, the one named last changes fastest.
Arguments:
- carried: bfloat16 [3072, 4096], P('dp', 'ra'), may hold values from -100 to 100
- branch_in: bfloat16 [3072, 4096], P('dp', 'ra'), may hold values from -12 to 12
- gain_in: float32 [4096], P('ra'), may hold values from 0.1 to 1.9
- bias_in: float32 [4096], P('ra'), may hold values from -1.8 to 1.8
- up_weight: bfloat16 [4096, 16384], P('ra', 'cb'), may hold values from -0.125 to 0.125
- down_weight: bfloat16 [16384, 4096], P('cb', 'ra'), may hold values from -0.046875 to 0.046875
- gain_out: float32 [4096], P('ra'), may hold values from 0.1 to 1.9
- bias_out: float32 [4096], P('ra'), may hold values from -1.8 to 1.8
Outputs:
- layer_out: bfloat16 [3072, 4096], P('dp', 'ra')
All inputs are finite; a program needn't handle non-finite values.
Results may differ from a plain program's by a relative error of at most 0.006.
Values may be sent and summed in bfloat16 or wider, within the bound.
A program may use at most 64 MiB of HBM per device.

v0:
```python
import jax
import jax.numpy as jnp
from jax import lax
from jax.sharding import PartitionSpec as P

residual_scale = 2.0**0.25
norm_eps = 1e-05


def copy_for_each(array, axis):
    length = lax.axis_size(axis)
    return lax.all_to_all(
        jnp.broadcast_to(array[None], (length, *array.shape)), axis, 0, 0, tiled=True
    )


def of_everyone(array, axis):
    return copy_for_each(array, axis).sum(axis=0)


def packed_total(arrays, axis):
    ravelled, at, done = (jnp.concatenate([a.reshape(-1) for a in arrays]), 0, [])
    running = of_everyone(ravelled, axis)
    for a in arrays:
        done.append(running[at : at + a.size].reshape(a.shape))
        at += a.size
    return tuple(done)


def taken_together(array, axis):
    return copy_for_each(array, axis).astype(jnp.float32).sum(axis=0)


def normalize(mixed, totals, squares, width, gain, bias):
    mean = totals[:, None] / width
    spread = squares[:, None] / width - mean * mean
    return (mixed - mean) * lax.rsqrt(spread + norm_eps) * gain + bias


def per_device(carried, branch_in, gain_in, bias_in, up_weight, down_weight, gain_out, bias_out):
    width = carried.shape[1] * lax.axis_size("ra")
    mixed_in = residual_scale * carried.astype(jnp.float32) + branch_in.astype(jnp.float32)
    totals, squares = packed_total(
        (jnp.sum(mixed_in, axis=1), jnp.sum(mixed_in * mixed_in, axis=1)), "ra"
    )
    normed = normalize(mixed_in, totals, squares, width, gain_in, bias_in).astype(jnp.bfloat16)
    regrouped = lax.all_to_all(up_weight, "ra", split_axis=1, concat_axis=0, tiled=True)
    pre_share = lax.dot_general(
        regrouped,
        lax.all_gather(normed, "ra", axis=1, tiled=True),
        (((0,), (1,)), ((), ())),
        preferred_element_type=jnp.float32,
    )
    hidden_share = jnp.square(jnp.maximum(pre_share, 0.0)).astype(jnp.bfloat16)
    branch_part = lax.dot_general(
        lax.all_gather(hidden_share, "ra", axis=0, tiled=True),
        down_weight,
        (((0,), (0,)), ((), ())),
        preferred_element_type=jnp.float32,
    )
    branch_out = taken_together(branch_part.astype(jnp.bfloat16), "cb").astype(jnp.float32)
    mixed_out = residual_scale * normed.astype(jnp.float32) + branch_out
    totals_out, squares_out = packed_total(
        (jnp.sum(mixed_out, axis=1), jnp.sum(mixed_out * mixed_out, axis=1)), "ra"
    )
    return normalize(mixed_out, totals_out, squares_out, width, gain_out, bias_out).astype(
        jnp.bfloat16
    )


def solution(mesh):
    in_specs = (
        P("dp", "ra"),
        P("dp", "ra"),
        P("ra"),
        P("ra"),
        P("ra", "cb"),
        P("cb", "ra"),
        P("ra"),
        P("ra"),
    )
    out_specs = P("dp", "ra")
    return jax.shard_map(
        per_device, mesh=mesh, in_specs=in_specs, out_specs=out_specs, check_vma=False
    )
```

profile of v0, /device:TPU:0, one launch (start us, length us, event | category | flops | bytes accessed | tf_op | source)
XLA Modules:
  0.0 324.9 jit_solution(11136814874928397678)
XLA Ops:
  6.5 0.0 copy-start
  6.5 0.0 copy-start.3
  6.5 0.0 copy-start.4
  6.5 0.0 copy-start.5
  6.5 0.0 all-gather.3.cloned.1.call-start
  6.6 2.1 fusion.3
  8.7 0.1 broadcast_in_dim.6
  8.8 16.1 %all_to_all.36 = f32[16,1,3072]{2,1,0:T(1,128)S(1)} all-to-all(f32[16,1,3072]{2,1,0:T(1,128)S(1)} %broadcast_in_dim.6), channel_id=1, replica_groups=mesh['ra'=16,'cb'=4,'dp'=2] {'ra'}, dimensions={0} | all-to-all | bytes 393216 | tf_op jit(solution)/shard_map/all_to_all | solution.py:12
  24.9 0.1 reduce_sum.65
  25.1 0.0 copy-done.3
  25.1 0.0 copy-done.4
  25.1 0.0 copy-done.5
  25.1 2.5 add_convert_fusion.1
  27.6 0.0 all-gather.3.cloned.1.call-update
  27.6 0.0 all-gather.5.cloned.1.call-start
  27.7 4.1 %copy.14 = bf16[256,4096]{0,1:T(8,128)(2,1)} copy(bf16[256,4096]{1,0:T(8,128)(2,1)} %param.12) | data formatting | bytes 4194304 | tf_op args[4]
  31.7 44.3 %all_to_all.37 = bf16[256,16,256]{0,2,1:T(8,128)(2,1)} all-to-all(bf16[256,16,256]{0,2,1:T(8,128)(2,1)} %bitcast.10), channel_id=1, replica_groups=mesh['ra'=16,'cb'=4,'dp'=2] {'ra'}, dimensions={1} | all-to-all | bytes 4194304 | tf_op jit(solution)/shard_map/all_to_all | solution.py:47
  76.0 3.9 %copy.15 = bf16[16,256,256]{2,1,0:T(8,128)(2,1)} copy(bf16[16,256,256]{1,2,0:T(8,128)(2,1)} %bitcast.9) | data formatting | bytes 4194304 | tf_op jit(solution)/shard_map/all_to_all | solution.py:47
  79.9 65.2 %all-gather.3.cloned.1.call-done = bf16[1536,4096]{1,0:T(8,128)(2,1)} async-done(((bf16[1536,256]{1,0:T(8,128)(2,1)}), bf16[1536,4096]{1,0:T(8,128)(2,1)}) %all-gather.3.cloned.1.call-update) | async-done | bytes 12582928 | tf_op jit(solution)/shard_map/all_gather | solution.py:50
  145.1 9.6 %fusion.2 = bf16[256,1536]{0,1:T(8,128)(2,1)} fusion(bf16[1536,4096]{1,0:T(8,128)(2,1)} %all-gather.3.cloned.1.call-done, bf16[4096,256]{1,0:T(8,128)(2,1)} %bitcast.11), kind=kOutput, calls=%fused_computation.5 | convolution fusion | flops 3222405120 | bytes 15466496 | tf_op jit(solution)/shard_map/dot_general | solution.py:48
  154.7 0.0 all-gather.5.cloned.1.call-update
  154.7 98.0 %all-gather.5.cloned.1.call-done = bf16[4096,1536]{0,1:T(8,128)(2,1)} async-done(((bf16[256,1536]{0,1:T(8,128)(2,1)}), bf16[4096,1536]{0,1:T(8,128)(2,1)}) %all-gather.5.cloned.1.call-update) | async-done | bytes 12582928 | tf_op jit(solution)/shard_map/all_gather | solution.py:56
  252.8 0.0 copy-done
  252.8 6.5 %convolution_convert_fusion = bf16[1536,256]{1,0:T(8,128)(2,1)S(1)} fusion(bf16[4096,1536]{0,1:T(8,128)(2,1)} %all-gather.5.cloned.1.call-done, bf16[4096,256]{1,0:T(8,128)(2,1)S(1)} %copy-done), kind=kOutput, calls=%fused_computation.4 | convolution fusion | flops 3221618688 | bytes 15466496 | tf_op jit(solution)/shard_map/dot_general | solution.py:55
  259.3 0.2 broadcast_in_dim.7
  259.5 40.3 %all_to_all.38 = bf16[4,1536,256]{2,1,0:T(8,128)(2,1)S(1)} all-to-all(bf16[4,1536,256]{2,1,0:T(8,128)(2,1)S(1)} %broadcast_in_dim.7), channel_id=1, replica_groups=mesh['ra'=16,'cb'=4,'dp'=2] {'cb'}, dimensions={0} | all-to-all | bytes 6291456 | tf_op jit(solution)/shard_map/all_to_all | solution.py:12
  299.8 0.0 copy-start.2
  299.8 0.5 convert_reduce_fusion
  300.2 0.0 copy-start.1
  300.2 1.1 copy-done.1
  301.4 0.0 copy-done.2
  301.4 0.0 copy-start.6
  301.4 0.0 copy-start.7
  301.4 0.5 fusion.4
  301.9 0.1 broadcast_in_dim.8
  302.0 13.1 %all_to_all.39 = f32[16,1,3072]{2,1,0:T(1,128)S(1)} all-to-all(f32[16,1,3072]{2,1,0:T(1,128)S(1)} %broadcast_in_dim.8), channel_id=1, replica_groups=mesh['ra'=16,'cb'=4,'dp'=2] {'ra'}, dimensions={0} | all-to-all | bytes 393216 | tf_op jit(solution)/shard_map/all_to_all | solution.py:12
  315.1 0.1 reduce_sum.69
  315.3 0.0 copy-done.6
  315.3 0.0 copy-done.7
  315.3 2.8 add_convert_fusion
  (4 shorter events, 0.0 us)
Async XLA Ops:
  6.5 246.2 %copy-start = (bf16[4096,256]{1,0:T(8,128)(2,1)S(1)}, bf16[4096,256]{1,0:T(8,128)(2,1)}, u32[]{:S(2)}) copy-start(bf16[4096,256]{1,0:T(8,128)(2,1)} %param.13) | copy-start | bytes 6291460
  6.5 18.5 %copy-start.3 = (bf16[1536,256]{1,0:T(8,128)(2,1)S(1)}, bf16[1536,256]{1,0:T(8,128)(2,1)}, u32[]{:S(2)}) copy-start(bf16[1536,256]{1,0:T(8,128)(2,1)} %param.9) | copy-start | bytes 2359300
  6.5 18.5 %copy-start.4 = (f32[256]{0:T(256)S(1)}, f32[256]{0:T(256)}, u32[]{:S(2)}) copy-start(f32[256]{0:T(256)} %param.11) | copy-start | bytes 3076
  6.5 18.5 %copy-start.5 = (f32[256]{0:T(256)S(1)}, f32[256]{0:T(256)}, u32[]{:S(2)}) copy-start(f32[256]{0:T(256)} %param.10) | copy-start | bytes 3076
  6.5 138.6 %all-gather.3.cloned.1.call-start = ((), (), s32[]{:S(2)}) async-start(), calls=%async_computation.4 | async-start | bytes 13369344 | tf_op jit(solution)/shard_map/all_gather | solution.py:50
  27.6 225.1 %all-gather.5.cloned.1.call-start = ((), (), s32[]{:S(2)}) async-start(), calls=%async_computation.5 | async-start | bytes 13369344 | tf_op jit(solution)/shard_map/all_gather | solution.py:56
  299.8 1.6 copy-start.2
  300.2 1.2 copy-start.1
  301.4 13.9 %copy-start.6 = (f32[256]{0:T(256)S(1)}, f32[256]{0:T(256)}, u32[]{:S(2)}) copy-start(f32[256]{0:T(256)} %param.15) | copy-start | bytes 3076
  301.4 13.9 %copy-start.7 = (f32[256]{0:T(256)S(1)}, f32[256]{0:T(256)}, u32[]{:S(2)}) copy-start(f32[256]{0:T(256)} %param.14) | copy-start | bytes 3076
Sparse Core Ops, SparseCore 0:
  27.7 117.3 all-gather.2
  154.9 97.8 all-gather.4
where the time goes:
time: 325 us
  waiting for transfers between devices  163 us (50%)
  blocking collectives  114 us (35%)
  matrix products  16.1 us (5%)
  between operations  13.5 us (4%)
  local copies, waits for them, and re-layouts  9.57 us (3%)
  other arithmetic  8.59 us (3%)
    all_gather x1, waiting for transfers between devices, per_device(): lax.all_gather(hidden_share, 'ra', axis=0, tiled=True)  98 us
    all_to_all x3, blocking collectives, copy_for_each(): lax.all_to_all(jnp.broadcast_to(array[None], (length, *array.shape)), axi...  69.5 us
    all_gather x1, waiting for transfers between devices, per_device(): lax.all_gather(normed, 'ra', axis=1, tiled=True)  65.2 us
    all_to_all x1, blocking collectives, per_device(): lax.all_to_all(up_weight, 'ra', split_axis=1, concat_axis=0, tiled=True)  44.3 us
    dot_general x1, matrix products, per_device(): lax.dot_general(regrouped, lax.all_gather(normed, 'ra', axis=1, tiled=Tru...  9.57 us
  transfers between devices with their start and end apart: 2, of which 2 were waited for; matrix products, arithmetic and copies ran while one was open for 2% of the time, Pallas kernels for 0%

commit v1 on v0

v1 whole, which is shorter than its diff:
```python
import functools

import jax
import jax.numpy as jnp
from jax import lax
from jax.experimental import pallas as pl
from jax.experimental.pallas import tpu as pltpu
from jax.sharding import PartitionSpec as P

residual_scale = 2.0**0.25
norm_eps = 1e-05
MESH = pl.DeviceIdType.MESH
BF = jnp.bfloat16
F32 = jnp.float32

Q = 96
G = 4 * Q
W = 256
D = 16 * W
FS = 1024


def kernel(
    car, bra, gi, bi, wu_in, wd_in, go, bo, out,
    cbuf, bbuf, nloc, nb, wu, wd, hid, pf, pb, opp_p, opp_m, sum_p, sum_m,
    from_m, from_p, rsum, xsend, xrecv, mo, obuf,
    sx_s, sx_r, sz_s, sz_r, tx_s, tx_r, tz_s, tz_r,
    send_sem, recv_sem, local_sem,
):
    r = lax.axis_index("ra")
    y = lax.axis_index("cb")
    c = lax.axis_index("dp")
    z = lax.div(r, 4)
    x = lax.rem(r, 4)

    def turn(i, d):
        return lax.rem(i + d + 4, 4)

    def at_x(d):
        return (z * 4 + turn(x, d), y, c)

    def at_z(d):
        return (turn(z, d) * 4 + x, y, c)

    def at_y(d):
        return (r, turn(y, d), c)

    partner = (r, y, 1 - c)
    remote = []
    local = []

    def send(src, dst, device):
        k = len(remote)
        copy = pltpu.make_async_remote_copy(
            src_ref=src, dst_ref=dst, send_sem=send_sem.at[k], recv_sem=recv_sem.at[k],
            device_id=device, device_id_type=MESH,
        )
        copy.start()
        remote.append(copy)
        return copy

    def fetch(src, dst):
        k = len(local)
        copy = pltpu.make_async_copy(src, dst, local_sem.at[k])
        copy.start()
        local.append(copy)
        return copy

    class Ring:
        def __init__(self, pos, dev, blk):
            self.pos, self.dev, self.blk = pos, dev, blk

        def start(self):
            mine = self.blk(self.pos, None)
            self.p = send(mine, mine, self.dev(1))
            self.m = send(mine, mine, self.dev(-1))

        def forward(self):
            self.p.wait_recv()
            half = self.blk(turn(self.pos, -1), 0)
            self.fp = send(half, half, self.dev(1))
            self.m.wait_recv()
            half = self.blk(turn(self.pos, 1), 1)
            self.fm = send(half, half, self.dev(-1))

        def finish(self):
            self.fp.wait_recv()
            self.fm.wait_recv()

    def rows(start, size, step):
        return pl.ds(pl.multiple_of(start, step), size)

    load_c = fetch(car.at[:, y], cbuf)
    load_b = fetch(bra.at[:, y], bbuf)

    def wrow(zz, xx, cc):
        return (lax.div(zz, 2) * 4 + xx) * 512 + lax.rem(zz, 2) * 256 + cc * 128

    def wblk(zz, xx, half=None):
        start = wrow(zz, xx, c)
        if half is None:
            return wu.at[rows(start, 128, 128), :]
        return wu.at[rows(start + half * 64, 64, 64), :]

    load_wu = fetch(
        wu_in.at[rows(c * 128, 128, 128), rows(x * FS, FS, FS)], wblk(z, x)
    )
    wd_half = rows(c * 512, 512, 512)
    load_wd = fetch(wd_in.at[rows(x * FS + c * 512, 512, 512), :], wd.at[x, wd_half, :])

    barrier = pltpu.get_barrier_semaphore()
    friends = [at_x(1), at_x(2), at_x(3), at_z(1), at_z(2), at_z(3), at_y(1), at_y(3), partner]
    for device in friends:
        pl.semaphore_signal(barrier, inc=1, device_id=device, device_id_type=MESH)

    def mixed_of(i):
        return residual_scale * cbuf[i].astype(F32) + bbuf[i].astype(F32)

    def sums_of(mixed):
        total = jnp.sum(mixed, axis=1, keepdims=True)
        square = jnp.sum(mixed * mixed, axis=1, keepdims=True)
        lane = lax.broadcasted_iota(jnp.int32, (G, 128), 1)
        return jnp.transpose(jnp.where(lane == 0, total, square))[0:8]

    def columns_of(totals):
        row = lax.broadcasted_iota(jnp.int32, (128, G), 0)
        spread = jnp.transpose(jnp.where(row == 0, totals[0:1], totals[1:2]))
        mean = spread[:, 0:1] / D
        var = spread[:, 1:2] / D - mean * mean
        return mean, lax.rsqrt(var + norm_eps)

    def exchange_start(buf, own, got, dev):
        buf[...] = own
        return [send(buf, got.at[d - 1], dev(d)) for d in (1, 2, 3)]

    def exchange_end(copies, buf, got):
        for copy in copies:
            copy.wait_recv()
        return buf[...] + got[0] + got[1] + got[2]

    load_c.wait()
    load_b.wait()
    mixed_in = jnp.concatenate([mixed_of(i) for i in range(4)], axis=0)
    own_sums = sums_of(mixed_in)
    pl.semaphore_wait(barrier, len(friends))

    stat = exchange_start(sx_s, own_sums, sx_r, at_x)
    a2a = {}
    for d in (1, 3, 2):
        to = turn(x, d)
        a2a[d] = send(
            wu_in.at[rows(c * 128, 128, 128), rows(to * FS, FS, FS)], wblk(z, x), at_x(d)
        )
    part = exchange_end(stat, sx_s, sx_r)
    stat = exchange_start(sz_s, part, sz_r, at_z)

    d2d = []

    def share(zz, xx):
        d2d.append(send(wblk(zz, xx), wblk(zz, xx), partner))

    def wring(u):
        xx = turn(x, -u)
        return Ring(z, at_z, lambda i, half: wblk(i, xx, half))

    wrings = {u: wring(u) for u in range(4)}
    load_wu.wait()
    wrings[0].start()
    share(z, x)

    totals = exchange_end(stat, sz_s, sz_r)
    mean, scale = columns_of(totals)
    normed = (
        (jnp.concatenate([mixed_of(i) for i in range(4)], axis=0) - mean) * scale * gi[...]
        + bi[...]
    ).astype(BF)
    for i in range(4):
        nloc[i] = normed[i * Q : (i + 1) * Q]

    ncol = (lax.div(z, 2) * 4 + x) * 512 + lax.rem(z, 2) * 256
    mine = nb.at[rows(y * Q, Q, 32), rows(ncol, W, W)]
    nsend = []
    for d in (1, 3, 2):
        nsend.append(send(nloc.at[turn(z, d)], mine, at_z(d)))
    nb[rows(y * Q, Q, 32), rows(ncol, W, W)] = nloc[z]

    for u in (1, 3):
        a2a[u].wait_recv()
        wrings[u].start()
        share(z, turn(x, -u))

    for copy in nsend:
        copy.wait_recv()

    def ablk1(i, half):
        col, size = (i * 512, 512) if half is None else (i * 512 + half * 256, 256)
        return nb.at[rows(y * Q, Q, 32), rows(col, size, 256)]

    def bblk1(i, half):
        col, size = (2048 + x * 512, 512) if half is None else (2048 + x * 512 + half * 256, 256)
        return nb.at[rows(i * Q, Q, 32), rows(col, size, 256)]

    def ablk2(i, half):
        cols = pl.ds(0, 2048) if half is None else pl.ds(half * 1024, 1024)
        return nb.at[rows(i * Q, Q, 32), cols]

    def bblk2(i, half):
        col, size = (2048 + i * 512, 512) if half is None else (2048 + i * 512 + half * 256, 256)
        return nb.at[:, rows(col, size, 256)]

    a1, b1 = Ring(x, at_x, ablk1), Ring(y, at_y, bblk1)
    a2, b2 = Ring(y, at_y, ablk2), Ring(x, at_x, bblk2)
    a1.start()
    b1.start()
    a2a[2].wait_recv()
    wrings[2].start()
    share(z, turn(x, -2))
    b1.forward()
    a1.forward()
    b1.finish()
    b2.start()
    a1.finish()
    a2.start()

    wd_a2a = []
    for d in (1, 3, 2):
        to = turn(x, d)
        wd_a2a.append(
            send(wd_in.at[rows(to * FS + c * 512, 512, 512), :], wd.at[x, wd_half, :], at_x(d))
        )

    for u in (0, 1, 3, 2):
        wrings[u].forward()
        share(turn(z, -1), turn(x, -u))
        share(turn(z, 1), turn(x, -u))
    b2.forward()
    a2.forward()
    for u in (0, 1, 3, 2):
        wrings[u].finish()
        share(turn(z, 2), turn(x, -u))
    load_wd.wait()
    wshare = [send(wd.at[x, wd_half, :], wd.at[x, wd_half, :], partner)]
    for copy, d in zip(wd_a2a, (1, 3, 2)):
        copy.wait_recv()
        at = wd.at[turn(x, -d), wd_half, :]
        wshare.append(send(at, at, partner))
    b2.finish()
    a2.finish()
    for copy in d2d:
        copy.wait_recv()

    hrings = []
    for n in range(4):
        cols = slice(n * 256, (n + 1) * 256)
        pre = jnp.dot(nb[...], wu[:, cols], preferred_element_type=F32)
        hid[z, :, cols] = jnp.square(jnp.maximum(pre, 0.0)).astype(BF)

        def hblk(i, half, n=n):
            if half is None:
                return hid.at[i, :, pl.ds(n * 256, 256)]
            return hid.at[i, pl.ds(half * 192, 192), pl.ds(n * 256, 256)]

        hrings.append(Ring(z, at_z, hblk))
        hrings[n].start()
    for copy in wshare:
        copy.wait_recv()

    def down(k, group):
        for j in range(4):
            part = jnp.dot(hid[group], wd[j], preferred_element_type=F32)
            pf[k, j] = part
            pb[k, j] = part.astype(BF)

    yp, ym = turn(y, 1), turn(y, -1)

    def quarter(ref, k, q, half):
        return ref.at[k, pl.ds(half * 2, 2), rows(q * Q, Q, 32), :]

    state = {}

    def y_first(k):
        q = turn(y, 2)
        s = {}
        s["op"] = send(quarter(pb, k, q, 0), opp_p.at[k], at_y(1))
        s["om"] = send(quarter(pb, k, q, 1), opp_m.at[k], at_y(-1))
        s["dp"] = send(quarter(pb, k, yp, 1), from_m.at[k, pl.ds(2, 2)], at_y(1))
        s["dm"] = send(quarter(pb, k, ym, 0), from_p.at[k, pl.ds(0, 2)], at_y(-1))
        state[k] = s

    def y_second(k):
        s = state[k]
        s["op"].wait_recv()
        sum_p[k] = (pf[k, 0:2, rows(yp * Q, Q, 32), :] + opp_p[k].astype(F32)).astype(BF)
        s["sp"] = send(sum_p.at[k], from_m.at[k, pl.ds(0, 2)], at_y(1))
        s["om"].wait_recv()
        sum_m[k] = (pf[k, 2:4, rows(ym * Q, Q, 32), :] + opp_m[k].astype(F32)).astype(BF)
        s["sm"] = send(sum_m.at[k], from_p.at[k, pl.ds(2, 2)], at_y(-1))

    def x_first(k):
        s = state[k]
        for name in ("dp", "dm", "sp", "sm"):
            s[name].wait_recv()
        total = (
            pf[k, :, rows(y * Q, Q, 32), :] + from_m[k].astype(F32) + from_p[k].astype(F32)
        )
        rsum[k] = total
        xsend[k] = total.astype(BF)
        s["x"] = [send(xsend.at[k, turn(x, d)], xrecv.at[k, d - 1], at_x(d)) for d in (1, 3, 2)]

    def x_second(k, group):
        for copy in state[k]["x"]:
            copy.wait_recv()
        branch = rsum[k, x]
        for d in range(3):
            branch = branch + xrecv[k, d].astype(F32)
        mo[group] = residual_scale * nloc[group].astype(F32) + branch

    groups = [z, turn(z, -1), turn(z, 1), turn(z, 2)]
    down(0, groups[0])
    y_first(0)
    for ring in hrings:
        ring.forward()
    y_second(0)
    down(1, groups[1])
    y_first(1)
    down(2, groups[2])
    y_first(2)
    x_first(0)
    y_second(1)
    y_second(2)
    for ring in hrings:
        ring.finish()
    down(3, groups[3])
    y_first(3)
    x_first(1)
    x_first(2)
    x_second(0, groups[0])
    y_second(3)
    x_second(1, groups[1])
    x_second(2, groups[2])
    x_first(3)
    x_second(3, groups[3])

    mixed_out = jnp.concatenate([mo[i] for i in range(4)], axis=0)
    stat = exchange_start(tx_s, sums_of(mixed_out), tx_r, at_x)
    part = exchange_end(stat, tx_s, tx_r)
    stat = exchange_start(tz_s, part, tz_r, at_z)
    totals = exchange_end(stat, tz_s, tz_r)
    mean, scale = columns_of(totals)
    mixed_out = jnp.concatenate([mo[i] for i in range(4)], axis=0)
    result = ((mixed_out - mean) * scale * go[...] + bo[...]).astype(BF)
    for i in range(4):
        obuf[y, i] = result[i * Q : (i + 1) * Q]

    def oblk(i, half):
        if half is None:
            return obuf.at[i]
        return obuf.at[i, pl.ds(half * 2, 2)]

    ring = Ring(y, at_y, oblk)
    ring.start()
    stores = [fetch(obuf.at[y], out.at[:, y])]
    ring.forward()
    stores.append(fetch(obuf.at[ym], out.at[:, ym]))
    stores.append(fetch(obuf.at[yp], out.at[:, yp]))
    ring.finish()
    far = turn(y, 2)
    stores.append(fetch(obuf.at[far], out.at[:, far]))
    assert len(remote) == N_REMOTE and len(local) == N_LOCAL
    for copy in remote:
        copy.wait_send()
    for copy in stores:
        copy.wait()


N_REMOTE = 129
N_LOCAL = 8


def per_device(carried, branch_in, gain_in, bias_in, up_weight, down_weight, gain_out, bias_out):
    any_spec = pl.BlockSpec(memory_space=pl.ANY)
    vmem_spec = pl.BlockSpec(memory_space=pltpu.VMEM)
    V = pltpu.VMEM
    result = pl.pallas_call(
        kernel,
        out_shape=jax.ShapeDtypeStruct((4, 4, Q, W), BF),
        in_specs=[any_spec, any_spec, vmem_spec, vmem_spec, any_spec, any_spec, vmem_spec, vmem_spec],
        out_specs=any_spec,
        scratch_shapes=[
            V((4, Q, W), BF), V((4, Q, W), BF), V((4, Q, W), BF),
            V((G, D), BF), V((D, FS), BF), V((4, FS, W), BF), V((4, G, FS), BF),
            V((4, 4, G, W), F32), V((4, 4, G, W), BF),
            V((4, 2, Q, W), BF), V((4, 2, Q, W), BF), V((4, 2, Q, W), BF), V((4, 2, Q, W), BF),
            V((4, 4, Q, W), BF), V((4, 4, Q, W), BF),
            V((4, 4, Q, W), F32), V((4, 4, Q, W), BF), V((4, 3, Q, W), BF),
            V((4, Q, W), F32), V((4, 4, Q, W), BF),
            V((8, G), F32), V((3, 8, G), F32), V((8, G), F32), V((3, 8, G), F32),
            V((8, G), F32), V((3, 8, G), F32), V((8, G), F32), V((3, 8, G), F32),
            pltpu.SemaphoreType.DMA((N_REMOTE,)),
            pltpu.SemaphoreType.DMA((N_REMOTE,)),
            pltpu.SemaphoreType.DMA((N_LOCAL,)),
        ],
        compiler_params=pltpu.CompilerParams(
            collective_id=0, has_side_effects=True, vmem_limit_bytes=60 * 1024 * 1024
        ),
    )(
        carried.reshape(4, 4, Q, W), branch_in.reshape(4, 4, Q, W),
        gain_in.reshape(1, W), bias_in.reshape(1, W), up_weight, down_weight,
        gain_out.reshape(1, W), bias_out.reshape(1, W),
    )
    return result.reshape(carried.shape)


def solution(mesh):
    in_specs = (
        P("dp", "ra"),
        P("dp", "ra"),
        P("ra"),
        P("ra"),
        P("ra", "cb"),
        P("cb", "ra"),
        P("ra"),
        P("ra"),
    )
    out_specs = P("dp", "ra")
    return jax.shard_map(
        per_device, mesh=mesh, in_specs=in_specs, out_specs=out_specs, check_vma=False
    )
```

time: 325 us -> 121 us (0.37)
  waiting for transfers between devices: 163 us -> 0 us
  Pallas kernels: 0 us -> 119 us
  blocking collectives: 114 us -> 0 us
  matrix products: 16.1 us -> 0 us
  between operations: 13.5 us -> 0.01 us
  other arithmetic: 8.59 us -> 0 us
  local copies, waits for them, and re-layouts: 9.57 us -> 2.06 us
    all_gather x2 -> x0, waiting for transfers between devices: 163 us -> none  [the longest x1 98 us: per_device(): lax.all_gather(hidden_share, 'ra', axis=0, tiled=True)]
    pallas_call x0 -> x1, Pallas kernels: none -> 119 us  [per_device(): pl.pallas_call(kernel, out_shape=jax.ShapeDtypeStruct((4, 4, Q, W), BF),...]
    all_to_all x4 -> x0, blocking collectives: 114 us -> none  [the longest x3 69.5 us: copy_for_each(): lax.all_to_all(jnp.broadcast_to(array[None], (length, *array.shape)), axi...]
    dot_general x2 -> x0, matrix products: 16.1 us -> none  [the longest x1 9.57 us: per_device(): lax.dot_general(regrouped, lax.all_gather(normed, 'ra', axis=1, tiled=Tru...]
    convert_element_type x2 -> x0, other arithmetic: 5.26 us -> none  [the longest x1 2.77 us: per_device(): normalize(mixed_out, totals_out, squares_out, width, gain_out, bias_out)]
    all_to_all x1 -> x0, local copies, waits for them, and re-layouts: 3.91 us -> none  [per_device(): lax.all_to_all(up_weight, 'ra', split_axis=1, concat_axis=0, tiled=True)]
    reduce_sum x5 -> x0, other arithmetic: 3.3 us -> none  [the longest x1 2.06 us: per_device(): jnp.sum(mixed_in, axis=1)]
  transfers between devices with their start and end apart: 2 -> 0, of which waited for: 2 -> 0; matrix products, arithmetic and copies ran while one was open for 2% -> 0% of each run, Pallas kernels for 0% -> 0%
where the time goes in v1:
time: 121 us
  Pallas kernels  119 us (98%)
  local copies, waits for them, and re-layouts  2.06 us (2%)
    pallas_call x1, Pallas kernels, per_device(): pl.pallas_call(kernel, out_shape=jax.ShapeDtypeStruct((4, 4, Q, W), BF),...  119 us

profile of v1, /device:TPU:0, one launch (start us, length us, event | category | flops | bytes accessed | tf_op | source)
XLA Modules:
  0.0 120.8 jit_solution(3168270317357514592)
XLA Ops:
  0.0 118.7 %shard_map.82 = bf16[4,4,96,256]{3,2,1,0:T(8,128)(2,1)} custom-call(bf16[4,4,96,256]{3,2,1,0:T(8,128)(2,1)} %bitcast.8, bf16[4,4,96,256]{3,2,1,0:T(8,128)(2,1)} %bitcast.9, f32[1,256]{1,0:T(1,128)} %bitcast.10, f32[1,256]{1,0:T(1,128)} %bitcast.11, bf16[256,4096]{1,0:T(8,128)(2,1)} %wu_in.1, bf16[4096,256]{1,0:T(8,128)(2,1)} %wd_in.1, f32[1,256]{1,0:T(1,128)} %bitcast.12, ...), custom_call_target="tpu_custom_call" | custom-call | tf_op jit(solution)/shard_map/pallas_call | solution.py:384
  118.8 2.1 %copy.10 = bf16[1536,256]{1,0:T(8,128)(2,1)} copy(bf16[1536,256]{1,0:T(8,128)(2,1)} %bitcast.7) | data formatting | bytes 1572864

commit v2 on v1

v2 whole, which is shorter than its diff:
```python
import functools

import jax
import jax.numpy as jnp
from jax import lax
from jax.experimental import pallas as pl
from jax.experimental.pallas import tpu as pltpu
from jax.sharding import PartitionSpec as P

residual_scale = 2.0**0.25
norm_eps = 1e-05
MESH = pl.DeviceIdType.MESH
BF = jnp.bfloat16
F32 = jnp.float32

Q = 96
G = 4 * Q
W = 256
D = 16 * W
FS = 1024


def kernel(
    car, bra, gi, bi, wu_in, wd_in, go, bo, out,
    cbuf, bbuf, nloc, nb, wu, wd, hid, pf, pb, opp_p, opp_m, sum_p, sum_m,
    from_m, from_p, rsum, tosend, torecv, mo, mob, obuf,
    sx_s, sx_r, sz_s, sz_r, tx_s, tx_r, tz_s, tz_r, totals, means, scales,
    send_sem, recv_sem, local_sem,
):
    r = lax.axis_index("ra")
    y = lax.axis_index("cb")
    c = lax.axis_index("dp")
    z = lax.div(r, 4)
    x = lax.rem(r, 4)

    def turn(i, d):
        return lax.rem(i + d + 4, 4)

    def at_x(d):
        return (z * 4 + turn(x, d), y, c)

    def at_z(d):
        return (turn(z, d) * 4 + x, y, c)

    def at_y(d):
        return (r, turn(y, d), c)

    partner = (r, y, 1 - c)
    remote = []
    local = []

    def send(src, dst, device):
        k = len(remote)
        copy = pltpu.make_async_remote_copy(
            src_ref=src, dst_ref=dst, send_sem=send_sem.at[k], recv_sem=recv_sem.at[k],
            device_id=device, device_id_type=MESH,
        )
        copy.start()
        remote.append(copy)
        return copy

    def fetch(src, dst):
        k = len(local)
        copy = pltpu.make_async_copy(src, dst, local_sem.at[k])
        copy.start()
        local.append(copy)
        return copy

    class Ring:
        def __init__(self, pos, dev, blk):
            self.pos, self.dev, self.blk = pos, dev, blk

        def start(self):
            mine = self.blk(self.pos, None)
            self.p = send(mine, mine, self.dev(1))
            self.m = send(mine, mine, self.dev(-1))

        def forward(self):
            self.p.wait_recv()
            half = self.blk(turn(self.pos, -1), 0)
            self.fp = send(half, half, self.dev(1))
            self.m.wait_recv()
            half = self.blk(turn(self.pos, 1), 1)
            self.fm = send(half, half, self.dev(-1))

        def finish(self):
            self.fp.wait_recv()
            self.fm.wait_recv()

    def rows(start, size, step):
        return pl.ds(pl.multiple_of(start, step), size)

    load_c = fetch(car.at[:, y], cbuf)
    load_b = fetch(bra.at[:, y], bbuf)

    def wrow(zz, xx, cc):
        return (lax.div(zz, 2) * 4 + xx) * 512 + lax.rem(zz, 2) * 256 + cc * 128

    def wblk(zz, xx, f, half=None):
        start = wrow(zz, xx, c)
        if half is None:
            return wu.at[rows(start, 128, 128), pl.ds(f * 512, 512)]
        return wu.at[rows(start + half * 64, 64, 64), pl.ds(f * 512, 512)]

    load_wu = fetch(
        wu_in.at[rows(c * 128, 128, 128), rows(x * FS, FS, FS)],
        wu.at[rows(wrow(z, x, c), 128, 128), :],
    )
    wd_half = rows(c * 512, 512, 512)
    load_wd = fetch(wd_in.at[rows(x * FS + c * 512, 512, 512), :], wd.at[x, wd_half, :])

    barrier = pltpu.get_barrier_semaphore()
    friends = [dev(d) for dev in (at_x, at_z, at_y) for d in (1, 2, 3)] + [partner]
    for device in friends:
        pl.semaphore_signal(barrier, inc=1, device_id=device, device_id_type=MESH)

    def mixed_of(i):
        return residual_scale * cbuf[i].astype(F32) + bbuf[i].astype(F32)

    def sums_of(mixed):
        total = jnp.sum(mixed, axis=1, keepdims=True)
        square = jnp.sum(mixed * mixed, axis=1, keepdims=True)
        lane = lax.broadcasted_iota(jnp.int32, (mixed.shape[0], 128), 1)
        return jnp.transpose(jnp.where(lane == 0, total, square))[0:8]

    def columns_of(sums):
        row = lax.broadcasted_iota(jnp.int32, (128, sums.shape[1]), 0)
        spread = jnp.transpose(jnp.where(row == 0, sums[0:1], sums[1:2]))
        mean = spread[:, 0:1] / D
        var = spread[:, 1:2] / D - mean * mean
        return mean, lax.rsqrt(var + norm_eps)

    def exchange_start(buf, own, got, dev):
        buf[...] = own
        return [send(buf, got.at[d - 1], dev(d)) for d in (1, 2, 3)]

    def exchange_end(copies, buf, got):
        for copy in copies:
            copy.wait_recv()
        return buf[...] + got[0] + got[1] + got[2]

    d2d = {0: [], 1: []}

    def share(zz, xx, f):
        d2d[f].append(send(wblk(zz, xx, f), wblk(zz, xx, f), partner))

    def wring(u, f):
        xx = turn(x, -u)
        return Ring(z, at_z, lambda i, half: wblk(i, xx, f, half))

    wrings = {(u, f): wring(u, f) for u in range(4) for f in range(2)}
    a2a = {}

    def wu_send(d, f):
        cols = rows(turn(x, d) * FS + f * 512, 512, 512)
        a2a[d, f] = send(wu_in.at[rows(c * 128, 128, 128), cols], wblk(z, x, f), at_x(d))

    def w_start(u, f):
        if u:
            a2a[u, f].wait_recv()
        wrings[u, f].start()
        share(z, turn(x, -u), f)

    def w_forward(u, f):
        wrings[u, f].forward()
        share(turn(z, -1), turn(x, -u), f)
        share(turn(z, 1), turn(x, -u), f)

    def w_finish(u, f):
        wrings[u, f].finish()
        share(turn(z, 2), turn(x, -u), f)

    load_c.wait()
    load_b.wait()
    mixed_in = jnp.concatenate([mixed_of(i) for i in range(4)], axis=0)
    own_sums = sums_of(mixed_in)
    load_wu.wait()
    pl.semaphore_wait(barrier, len(friends))

    stat = exchange_start(sx_s, own_sums, sx_r, at_x)
    w_start(0, 0)
    for d in (1, 3, 2):
        wu_send(d, 0)
    w_start(0, 1)
    wu_send(1, 1)
    wu_send(3, 1)
    part = exchange_end(stat, sx_s, sx_r)
    stat = exchange_start(sz_s, part, sz_r, at_z)
    w_start(1, 0)
    mean, scale = columns_of(exchange_end(stat, sz_s, sz_r))
    normed = (
        (jnp.concatenate([mixed_of(i) for i in range(4)], axis=0) - mean) * scale * gi[...]
        + bi[...]
    ).astype(BF)
    for i in range(4):
        nloc[i] = normed[i * Q : (i + 1) * Q]

    ncol = (lax.div(z, 2) * 4 + x) * 512 + lax.rem(z, 2) * 256
    mine = nb.at[rows(y * Q, Q, 32), rows(ncol, W, W)]
    nsend = []
    for d in (1, 3, 2):
        nsend.append(send(nloc.at[turn(z, d)], mine, at_z(d)))
    nb[rows(y * Q, Q, 32), rows(ncol, W, W)] = nloc[z]
    w_start(3, 0)
    w_forward(0, 0)
    for copy in nsend:
        copy.wait_recv()

    def nblk(h, xx, yy, part):
        col, size = h * 2048 + xx * 512, 512
        if part is not None:
            col, size = col + part * 256, 256
        return nb.at[rows(yy * Q, Q, 32), rows(col, size, 256)]

    a1 = Ring(x, at_x, lambda i, part: nblk(0, i, y, part))
    b1 = Ring(y, at_y, lambda i, part: nblk(1, x, i, part))

    def second(j):
        return (
            Ring(y, at_y, lambda i, part: nblk(0, turn(x, -j), i, part)),
            Ring(x, at_x, lambda i, part: nblk(1, i, turn(y, -j), part)),
        )

    seconds = [second(j) for j in range(4)]

    def n_start(j):
        for ring in seconds[j]:
            ring.start()

    def n_forward(j):
        for ring in seconds[j]:
            ring.forward()

    a1.start()
    b1.start()
    n_start(0)
    w_start(2, 0)
    w_forward(1, 0)
    b1.forward()
    a1.forward()
    n_start(1)
    n_start(3)
    wu_send(2, 1)
    w_start(1, 1)
    w_forward(3, 0)
    w_forward(0, 1)
    n_forward(0)
    b1.finish()
    a1.finish()
    n_start(2)
    w_start(3, 1)
    w_forward(2, 0)
    for u in (0, 1, 3):
        w_finish(u, 0)
    n_forward(1)
    w_forward(1, 1)
    w_start(2, 1)
    w_finish(2, 0)
    w_finish(0, 1)
    n_forward(3)
    w_forward(3, 1)
    n_forward(2)

    wd_a2a = []
    for d in (1, 3, 2):
        to = turn(x, d)
        wd_a2a.append(
            send(wd_in.at[rows(to * FS + c * 512, 512, 512), :], wd.at[x, wd_half, :], at_x(d))
        )
    load_wd.wait()
    wshare = [send(wd.at[x, wd_half, :], wd.at[x, wd_half, :], partner)]
    w_forward(2, 1)
    for pair in seconds:
        for ring in pair:
            ring.finish()
    for copy in d2d[0]:
        copy.wait_recv()

    hrings = []

    def up(n):
        cols = slice(n * 256, (n + 1) * 256)
        pre = jnp.dot(nb[...], wu[:, cols], preferred_element_type=F32)
        hid[z, :, cols] = jnp.square(jnp.maximum(pre, 0.0)).astype(BF)

        def hblk(i, half):
            if half is None:
                return hid.at[i, :, pl.ds(n * 256, 256)]
            return hid.at[i, pl.ds(half * 192, 192), pl.ds(n * 256, 256)]

        ring = Ring(z, at_z, hblk)
        ring.start()
        hrings.append(ring)

    up(0)
    for u in (1, 3, 2):
        w_finish(u, 1)
    up(1)
    for copy, d in zip(wd_a2a, (1, 3, 2)):
        copy.wait_recv()
        at = wd.at[turn(x, -d), wd_half, :]
        wshare.append(send(at, at, partner))
    for copy in d2d[1]:
        copy.wait_recv()
    up(2)
    up(3)
    for copy in wshare:
        copy.wait_recv()

    def down(k, group):
        for j in range(4):
            part = jnp.dot(hid[group], wd[j], preferred_element_type=F32)
            for i in range(4):
                pf[k, j, i] = part[i * Q : (i + 1) * Q]
                pb[k, j, i] = part[i * Q : (i + 1) * Q].astype(BF)

    class Reduce:
        def __init__(self, k, kind):
            self.at = (k, kind)
            self.k = k
            self.kind = kind
            self.pos, self.dev = ((y, at_y), (x, at_x))[kind]
            self.pos2, self.dev2 = ((x, at_x), (y, at_y))[kind]

        def item(self, to, first, count):
            if self.kind == 0:
                return (self.k, pl.ds(first, count), to, pl.ds(0, 48), slice(None))
            return (self.k, to, pl.ds(first, count), pl.ds(48, 48), slice(None))

        def first(self):
            far, p, m = turn(self.pos, 2), turn(self.pos, 1), turn(self.pos, -1)
            self.p, self.m = p, m
            self.op = send(pb.at[self.item(far, 0, 2)], opp_p.at[self.at], self.dev(1))
            self.om = send(pb.at[self.item(far, 2, 2)], opp_m.at[self.at], self.dev(-1))
            low, high = pl.ds(0, 2), pl.ds(2, 2)
            self.dp = send(
                pb.at[self.item(p, 2, 2)], from_m.at[(*self.at, high)], self.dev(1)
            )
            self.dm = send(
                pb.at[self.item(m, 0, 2)], from_p.at[(*self.at, low)], self.dev(-1)
            )

        def second(self):
            low, high = pl.ds(0, 2), pl.ds(2, 2)
            self.op.wait_recv()
            sum_p[self.at] = (pf[self.item(self.p, 0, 2)] + opp_p[self.at].astype(F32)).astype(BF)
            self.sp = send(sum_p.at[self.at], from_m.at[(*self.at, low)], self.dev(1))
            self.om.wait_recv()
            sum_m[self.at] = (pf[self.item(self.m, 2, 2)] + opp_m[self.at].astype(F32)).astype(BF)
            self.sm = send(sum_m.at[self.at], from_p.at[(*self.at, high)], self.dev(-1))

        def third(self):
            for copy in (self.dp, self.dm, self.sp, self.sm):
                copy.wait_recv()
            total = (
                pf[self.item(self.pos, 0, 4)]
                + from_m[self.at].astype(F32)
                + from_p[self.at].astype(F32)
            )
            rsum[self.at] = total
            tosend[self.at] = total.astype(BF)
            self.last = [
                send(
                    tosend.at[(*self.at, turn(self.pos2, d))],
                    torecv.at[(*self.at, d - 1)],
                    self.dev2(d),
                )
                for d in (1, 3, 2)
            ]

        def fourth(self, group):
            for copy in self.last:
                copy.wait_recv()
            branch = rsum[(*self.at, self.pos2)]
            for d in range(3):
                branch = branch + torecv[(*self.at, d)].astype(F32)
            part = slice(self.kind * 48, self.kind * 48 + 48)
            mixed = residual_scale * nloc[group, part].astype(F32) + branch
            mo[group, part] = mixed
            mob[y, self.k, part] = mixed.astype(BF)

    groups = [z, turn(z, -1), turn(z, 1), turn(z, 2)]
    reduces = [(Reduce(k, 0), Reduce(k, 1)) for k in range(4)]

    def first(k):
        down(k, groups[k])
        for one in reduces[k]:
            one.first()

    def second_(k):
        for one in reduces[k]:
            one.second()

    def third(k):
        for one in reduces[k]:
            one.third()

    def fourth(k):
        for one in reduces[k]:
            one.fourth(groups[k])

    first(0)
    hrings[0].forward()
    hrings[1].forward()
    second_(0)
    hrings[2].forward()
    third(0)
    hrings[3].forward()
    first(1)
    first(2)
    fourth(0)
    second_(1)
    second_(2)
    third(1)
    third(2)
    for ring in hrings:
        ring.finish()
    first(3)
    fourth(1)
    fourth(2)

    def mblk(i, half):
        if half is None:
            return mob.at[i, pl.ds(0, 3)]
        return mob.at[i, pl.ds(0, 3), pl.ds(half * 48, 48)]

    ring = Ring(y, at_y, mblk)
    ring.start()
    second_(3)
    third(3)
    ring.forward()
    fourth(3)
    mixed_out = jnp.concatenate([mo[i] for i in range(4)], axis=0)
    stat = exchange_start(tx_s, sums_of(mixed_out), tx_r, at_x)
    last = [send(mob.at[y, 3], mob.at[y, 3], at_y(d)) for d in (1, 3, 2)]
    part = exchange_end(stat, tx_s, tx_r)
    stat = exchange_start(tz_s, part, tz_r, at_z)
    ring.finish()
    for copy in last:
        copy.wait_recv()
    totals[y] = exchange_end(stat, tz_s, tz_r)
    stat = [send(totals.at[y], totals.at[y], at_y(d)) for d in (1, 3, 2)]
    stores = []

    def finish(yy):
        mean, scale = columns_of(totals[yy])
        for i in range(4):
            means[i] = jnp.broadcast_to(mean[i * Q : (i + 1) * Q], (Q, 128))
            scales[i] = jnp.broadcast_to(scale[i * Q : (i + 1) * Q], (Q, 128))
        for k in range(4):
            mean = means[groups[k]][:, 0:1]
            scale = scales[groups[k]][:, 0:1]
            block = (mob[yy, k].astype(F32) - mean) * scale * go[...] + bo[...]
            obuf[yy, k] = block.astype(BF)
            stores.append(fetch(obuf.at[yy, k], out.at[groups[k], yy]))

    finish(y)
    for copy, d in zip(stat, (1, 3, 2)):
        copy.wait_recv()
        finish(turn(y, -d))
    assert (len(remote), len(local)) == (N_REMOTE, N_LOCAL), (len(remote), len(local))
    for copy in remote:
        copy.wait_send()
    for copy in stores:
        copy.wait()


N_REMOTE = 230
N_LOCAL = 20


def per_device(carried, branch_in, gain_in, bias_in, up_weight, down_weight, gain_out, bias_out):
    any_spec = pl.BlockSpec(memory_space=pl.ANY)
    vmem_spec = pl.BlockSpec(memory_space=pltpu.VMEM)
    V = pltpu.VMEM
    result = pl.pallas_call(
        kernel,
        out_shape=jax.ShapeDtypeStruct((4, 4, Q, W), BF),
        in_specs=[any_spec, any_spec, vmem_spec, vmem_spec, any_spec, any_spec, vmem_spec, vmem_spec],
        out_specs=any_spec,
        scratch_shapes=[
            V((4, Q, W), BF), V((4, Q, W), BF), V((4, Q, W), BF),
            V((G, D), BF), V((D, FS), BF), V((4, FS, W), BF), V((4, G, FS), BF),
            V((4, 4, 4, Q, W), F32), V((4, 4, 4, Q, W), BF),
            *[V((4, 2, 2, 48, W), BF) for _ in range(4)],
            V((4, 2, 4, 48, W), BF), V((4, 2, 4, 48, W), BF),
            V((4, 2, 4, 48, W), F32), V((4, 2, 4, 48, W), BF), V((4, 2, 3, 48, W), BF),
            V((4, Q, W), F32), V((4, 4, Q, W), BF), V((4, 4, Q, W), BF),
            *[V(shape, F32) for shape in ((8, G), (3, 8, G)) * 4],
            V((4, 8, G), F32), V((4, Q, 128), F32), V((4, Q, 128), F32),
            pltpu.SemaphoreType.DMA((N_REMOTE,)),
            pltpu.SemaphoreType.DMA((N_REMOTE,)),
            pltpu.SemaphoreType.DMA((N_LOCAL,)),
        ],
        compiler_params=pltpu.CompilerParams(
            collective_id=0, has_side_effects=True, vmem_limit_bytes=60 * 1024 * 1024
        ),
    )(
        carried.reshape(4, 4, Q, W), branch_in.reshape(4, 4, Q, W),
        gain_in.reshape(1, W), bias_in.reshape(1, W), up_weight, down_weight,
        gain_out.reshape(1, W), bias_out.reshape(1, W),
    )
    return result.reshape(carried.shape)


def solution(mesh):
    in_specs = (
        P("dp", "ra"),
        P("dp", "ra"),
        P("ra"),
        P("ra"),
        P("ra", "cb"),
        P("cb", "ra"),
        P("ra"),
        P("ra"),
    )
    out_specs = P("dp", "ra")
    return jax.shard_map(
        per_device, mesh=mesh, in_specs=in_specs, out_specs=out_specs, check_vma=False
    )
```

time: 121 us -> 111 us (0.917)
  Pallas kernels: 119 us -> 109 us
    pallas_call x1, Pallas kernels: 119 us -> 109 us  [per_device(): pl.pallas_call(kernel, out_shape=jax.ShapeDtypeStruct((4, 4, Q, W), BF),...]
where the time goes in v2:
time: 111 us
  Pallas kernels  109 us (98%)
  local copies, waits for them, and re-layouts  2.06 us (2%)
    pallas_call x1, Pallas kernels, per_device(): pl.pallas_call(kernel, out_shape=jax.ShapeDtypeStruct((4, 4, Q, W), BF),...  109 us

profile of v2, /device:TPU:0, one launch (start us, length us, event | category | flops | bytes accessed | tf_op | source)
XLA Modules:
  0.0 110.9 jit_solution(13145678736845536476)
XLA Ops:
  0.0 108.8 %shard_map.82 = bf16[4,4,96,256]{3,2,1,0:T(8,128)(2,1)} custom-call(bf16[4,4,96,256]{3,2,1,0:T(8,128)(2,1)} %bitcast.8, bf16[4,4,96,256]{3,2,1,0:T(8,128)(2,1)} %bitcast.9, f32[1,256]{1,0:T(1,128)} %bitcast.10, f32[1,256]{1,0:T(1,128)} %bitcast.11, bf16[256,4096]{1,0:T(8,128)(2,1)} %wu_in.1, bf16[4096,256]{1,0:T(8,128)(2,1)} %wd_in.1, f32[1,256]{1,0:T(1,128)} %bitcast.12, ...), custom_call_target="tpu_custom_call" | custom-call | tf_op jit(solution)/shard_map/pallas_call | solution.py:476
  108.9 2.1 %copy.10 = bf16[1536,256]{1,0:T(8,128)(2,1)} copy(bf16[1536,256]{1,0:T(8,128)(2,1)} %bitcast.7) | data formatting | bytes 1572864

commit v3 on v2

--- a/solution.py
+++ b/solution.py
@@ -24,7 +24,7 @@
     car, bra, gi, bi, wu_in, wd_in, go, bo, out,
     cbuf, bbuf, nloc, nb, wu, wd, hid, pf, pb, opp_p, opp_m, sum_p, sum_m,
     from_m, from_p, rsum, tosend, torecv, mo, mob, obuf,
-    sx_s, sx_r, sz_s, sz_r, tx_s, tx_r, tz_s, tz_r, totals, means, scales,
+    sx_s, sx_r, sz_s, sz_r, tx_s, tx_r, tz_s, tz_r, totals,
     send_sem, recv_sem, local_sem,
 ):
     r = lax.axis_index("ra")
@@ -49,18 +49,32 @@
     remote = []
     local = []
 
-    def send(src, dst, device):
-        k = len(remote)
-        copy = pltpu.make_async_remote_copy(
-            src_ref=src, dst_ref=dst, send_sem=send_sem.at[k], recv_sem=recv_sem.at[k],
+    used = []
+
+    def channel():
+        used.append(len(used))
+        return used[-1]
+
+    def described(src, dst, device, slot, on):
+        return pltpu.make_async_remote_copy(
+            src_ref=src, dst_ref=dst, send_sem=send_sem.at[slot], recv_sem=recv_sem.at[on],
             device_id=device, device_id_type=MESH,
         )
+
+    def send(src, dst, device, on=None):
+        k = len(remote)
+        if k >= N_SEND:
+            remote[k - N_SEND].wait_send()
+        copy = described(src, dst, device, k % N_SEND, channel() if on is None else on)
         copy.start()
         remote.append(copy)
         return copy
 
-    def fetch(src, dst):
-        k = len(local)
+    def expect(on, cover):
+        described(cover, cover, partner, 0, on).wait_recv()
+
+    def fetch(src, dst, on=None):
+        k = len(local) if on is None else on
         copy = pltpu.make_async_copy(src, dst, local_sem.at[k])
         copy.start()
         local.append(copy)
@@ -76,16 +90,16 @@
             self.m = send(mine, mine, self.dev(-1))
 
         def forward(self):
+            self.on = channel()
             self.p.wait_recv()
             half = self.blk(turn(self.pos, -1), 0)
-            self.fp = send(half, half, self.dev(1))
+            send(half, half, self.dev(1), self.on)
             self.m.wait_recv()
             half = self.blk(turn(self.pos, 1), 1)
-            self.fm = send(half, half, self.dev(-1))
+            send(half, half, self.dev(-1), self.on)
 
         def finish(self):
-            self.fp.wait_recv()
-            self.fm.wait_recv()
+            expect(self.on, self.blk(turn(self.pos, 2), None))
 
     def rows(start, size, step):
         return pl.ds(pl.multiple_of(start, step), size)
@@ -132,17 +146,22 @@
 
     def exchange_start(buf, own, got, dev):
         buf[...] = own
-        return [send(buf, got.at[d - 1], dev(d)) for d in (1, 2, 3)]
-
-    def exchange_end(copies, buf, got):
-        for copy in copies:
-            copy.wait_recv()
+        on = channel()
+        for d in (1, 2, 3):
+            send(buf, got.at[d - 1], dev(d), on)
+        return on
+
+    def exchange_end(on, buf, got):
+        expect(on, got)
         return buf[...] + got[0] + got[1] + got[2]
 
-    d2d = {0: [], 1: []}
+    d2d = (channel(), channel())
 
     def share(zz, xx, f):
-        d2d[f].append(send(wblk(zz, xx, f), wblk(zz, xx, f), partner))
+        send(wblk(zz, xx, f), wblk(zz, xx, f), partner, d2d[f])
+
+    def shared(f):
+        expect(d2d[f], wu.at[pl.ds(0, D // 2), pl.ds(f * 512, 512)])
 
     def wring(u, f):
         xx = turn(x, -u)
@@ -197,14 +216,13 @@
 
     ncol = (lax.div(z, 2) * 4 + x) * 512 + lax.rem(z, 2) * 256
     mine = nb.at[rows(y * Q, Q, 32), rows(ncol, W, W)]
-    nsend = []
+    nsend = channel()
     for d in (1, 3, 2):
-        nsend.append(send(nloc.at[turn(z, d)], mine, at_z(d)))
+        send(nloc.at[turn(z, d)], mine, at_z(d), nsend)
     nb[rows(y * Q, Q, 32), rows(ncol, W, W)] = nloc[z]
     w_start(3, 0)
     w_forward(0, 0)
-    for copy in nsend:
-        copy.wait_recv()
+    expect(nsend, nloc.at[pl.ds(0, 3)])
 
     def nblk(h, xx, yy, part):
         col, size = h * 2048 + xx * 512, 512
@@ -261,20 +279,17 @@
     w_forward(3, 1)
     n_forward(2)
 
-    wd_a2a = []
+    wd_a2a, wshare = channel(), channel()
     for d in (1, 3, 2):
         to = turn(x, d)
-        wd_a2a.append(
-            send(wd_in.at[rows(to * FS + c * 512, 512, 512), :], wd.at[x, wd_half, :], at_x(d))
-        )
+        part = wd_in.at[rows(to * FS + c * 512, 512, 512), :]
+        send(part, wd.at[x, wd_half, :], at_x(d), wd_a2a)
     load_wd.wait()
-    wshare = [send(wd.at[x, wd_half, :], wd.at[x, wd_half, :], partner)]
     w_forward(2, 1)
     for pair in seconds:
         for ring in pair:
             ring.finish()
-    for copy in d2d[0]:
-        copy.wait_recv()
+    shared(0)
 
     hrings = []
 
@@ -296,16 +311,12 @@
     for u in (1, 3, 2):
         w_finish(u, 1)
     up(1)
-    for copy, d in zip(wd_a2a, (1, 3, 2)):
-        copy.wait_recv()
-        at = wd.at[turn(x, -d), wd_half, :]
-        wshare.append(send(at, at, partner))
-    for copy in d2d[1]:
-        copy.wait_recv()
+    expect(wd_a2a, wd.at[pl.ds(0, 3), wd_half, :])
+    send(wd.at[:, wd_half, :], wd.at[:, wd_half, :], partner, wshare)
+    shared(1)
     up(2)
     up(3)
-    for copy in wshare:
-        copy.wait_recv()
+    expect(wshare, wd.at[:, wd_half, :])
 
     def down(k, group):
         for j in range(4):
@@ -333,25 +344,26 @@
             self.op = send(pb.at[self.item(far, 0, 2)], opp_p.at[self.at], self.dev(1))
             self.om = send(pb.at[self.item(far, 2, 2)], opp_m.at[self.at], self.dev(-1))
             low, high = pl.ds(0, 2), pl.ds(2, 2)
-            self.dp = send(
-                pb.at[self.item(p, 2, 2)], from_m.at[(*self.at, high)], self.dev(1)
+            self.on_m, self.on_p, self.on_2 = channel(), channel(), channel()
+            send(
+                pb.at[self.item(p, 2, 2)], from_m.at[(*self.at, high)], self.dev(1), self.on_m
             )
-            self.dm = send(
-                pb.at[self.item(m, 0, 2)], from_p.at[(*self.at, low)], self.dev(-1)
+            send(
+                pb.at[self.item(m, 0, 2)], from_p.at[(*self.at, low)], self.dev(-1), self.on_p
             )
 
         def second(self):
             low, high = pl.ds(0, 2), pl.ds(2, 2)
             self.op.wait_recv()
             sum_p[self.at] = (pf[self.item(self.p, 0, 2)] + opp_p[self.at].astype(F32)).astype(BF)
-            self.sp = send(sum_p.at[self.at], from_m.at[(*self.at, low)], self.dev(1))
+            send(sum_p.at[self.at], from_m.at[(*self.at, low)], self.dev(1), self.on_m)
             self.om.wait_recv()
             sum_m[self.at] = (pf[self.item(self.m, 2, 2)] + opp_m[self.at].astype(F32)).astype(BF)
-            self.sm = send(sum_m.at[self.at], from_p.at[(*self.at, high)], self.dev(-1))
+            send(sum_m.at[self.at], from_p.at[(*self.at, high)], self.dev(-1), self.on_p)
 
         def third(self):
-            for copy in (self.dp, self.dm, self.sp, self.sm):
-                copy.wait_recv()
+            expect(self.on_m, from_m.at[self.at])
+            expect(self.on_p, from_p.at[self.at])
             total = (
                 pf[self.item(self.pos, 0, 4)]
                 + from_m[self.at].astype(F32)
@@ -359,18 +371,12 @@
             )
             rsum[self.at] = total
             tosend[self.at] = total.astype(BF)
-            self.last = [
-                send(
-                    tosend.at[(*self.at, turn(self.pos2, d))],
-                    torecv.at[(*self.at, d - 1)],
-                    self.dev2(d),
-                )
-                for d in (1, 3, 2)
-            ]
+            for d in (1, 3, 2):
+                to = turn(self.pos2, d)
+                send(tosend.at[(*self.at, to)], torecv.at[(*self.at, d - 1)], self.dev2(d), self.on_2)
 
         def fourth(self, group):
-            for copy in self.last:
-                copy.wait_recv()
+            expect(self.on_2, torecv.at[self.at])
             branch = rsum[(*self.at, self.pos2)]
             for d in range(3):
                 branch = branch + torecv[(*self.at, d)].astype(F32)
@@ -416,8 +422,10 @@
     for ring in hrings:
         ring.finish()
     first(3)
+    second_(3)
     fourth(1)
     fourth(2)
+    third(3)
 
     def mblk(i, half):
         if half is None:
@@ -426,47 +434,43 @@
 
     ring = Ring(y, at_y, mblk)
     ring.start()
-    second_(3)
-    third(3)
-    ring.forward()
     fourth(3)
-    mixed_out = jnp.concatenate([mo[i] for i in range(4)], axis=0)
+    pad = jnp.zeros((32, W), F32)
+    mixed_out = jnp.concatenate([a for i in range(4) for a in (mo[i], pad)], axis=0)
     stat = exchange_start(tx_s, sums_of(mixed_out), tx_r, at_x)
-    last = [send(mob.at[y, 3], mob.at[y, 3], at_y(d)) for d in (1, 3, 2)]
+    last = channel()
+    for d in (1, 3, 2):
+        send(mob.at[y, 3], mob.at[y, 3], at_y(d), last)
     part = exchange_end(stat, tx_s, tx_r)
     stat = exchange_start(tz_s, part, tz_r, at_z)
+    ring.forward()
     ring.finish()
-    for copy in last:
-        copy.wait_recv()
+    expect(last, mob.at[pl.ds(0, 3), 3])
     totals[y] = exchange_end(stat, tz_s, tz_r)
-    stat = [send(totals.at[y], totals.at[y], at_y(d)) for d in (1, 3, 2)]
-    stores = []
+    stat = channel()
+    for d in (1, 3, 2):
+        send(totals.at[y], totals.at[y], at_y(d), stat)
 
     def finish(yy):
-        mean, scale = columns_of(totals[yy])
-        for i in range(4):
-            means[i] = jnp.broadcast_to(mean[i * Q : (i + 1) * Q], (Q, 128))
-            scales[i] = jnp.broadcast_to(scale[i * Q : (i + 1) * Q], (Q, 128))
         for k in range(4):
-            mean = means[groups[k]][:, 0:1]
-            scale = scales[groups[k]][:, 0:1]
-            block = (mob[yy, k].astype(F32) - mean) * scale * go[...] + bo[...]
+            mean, scale = columns_of(totals[yy, :, rows(groups[k] * 128, 128, 128)])
+            block = (mob[yy, k].astype(F32) - mean[0:Q]) * scale[0:Q] * go[...] + bo[...]
             obuf[yy, k] = block.astype(BF)
-            stores.append(fetch(obuf.at[yy, k], out.at[groups[k], yy]))
+            fetch(obuf.at[yy, k], out.at[groups[k], yy], 4)
 
     finish(y)
-    for copy, d in zip(stat, (1, 3, 2)):
-        copy.wait_recv()
+    expect(stat, totals.at[pl.ds(0, 3)])
+    for d in (1, 3, 2):
         finish(turn(y, -d))
-    assert (len(remote), len(local)) == (N_REMOTE, N_LOCAL), (len(remote), len(local))
-    for copy in remote:
+    assert len(used) == N_RECV, len(used)
+    for copy in remote[-N_SEND:]:
         copy.wait_send()
-    for copy in stores:
-        copy.wait()
-
-
-N_REMOTE = 230
-N_LOCAL = 20
+    pltpu.make_async_copy(obuf, out, local_sem.at[4]).wait()
+
+
+N_SEND = 64
+N_RECV = 126
+N_LOCAL = 5
 
 
 def per_device(carried, branch_in, gain_in, bias_in, up_weight, down_weight, gain_out, bias_out):
@@ -486,10 +490,11 @@
             V((4, 2, 4, 48, W), BF), V((4, 2, 4, 48, W), BF),
             V((4, 2, 4, 48, W), F32), V((4, 2, 4, 48, W), BF), V((4, 2, 3, 48, W), BF),
             V((4, Q, W), F32), V((4, 4, Q, W), BF), V((4, 4, Q, W), BF),
-            *[V(shape, F32) for shape in ((8, G), (3, 8, G)) * 4],
-            V((4, 8, G), F32), V((4, Q, 128), F32), V((4, Q, 128), F32),
-            pltpu.SemaphoreType.DMA((N_REMOTE,)),
-            pltpu.SemaphoreType.DMA((N_REMOTE,)),
+            *[V(shape, F32) for shape in ((8, G), (3, 8, G)) * 2],
+            *[V(shape, F32) for shape in ((8, 512), (3, 8, 512)) * 2],
+            V((4, 8, 512), F32),
+            pltpu.SemaphoreType.DMA((N_SEND,)),
+            pltpu.SemaphoreType.DMA((N_RECV,)),
             pltpu.SemaphoreType.DMA((N_LOCAL,)),
         ],
         compiler_params=pltpu.CompilerParams(

time: 111 us -> 107 us (0.964)
  Pallas kernels: 109 us -> 105 us
    pallas_call x1, Pallas kernels: 109 us -> 105 us  [per_device(): pl.pallas_call(kernel, out_shape=jax.ShapeDtypeStruct((4, 4, Q, W), BF),...]
where the time goes in v3:
time: 107 us
  Pallas kernels  105 us (98%)
  local copies, waits for them, and re-layouts  2.06 us (2%)
    pallas_call x1, Pallas kernels, per_device(): pl.pallas_call(kernel, out_shape=jax.ShapeDtypeStruct((4, 4, Q, W), BF),...  105 us

profile of v3, /device:TPU:0, one launch (start us, length us, event | category | flops | bytes accessed | tf_op | source)
XLA Modules:
  0.0 106.8 jit_solution(9915988313744402859)
XLA Ops:
  0.0 104.7 %shard_map.82 = bf16[4,4,96,256]{3,2,1,0:T(8,128)(2,1)} custom-call(bf16[4,4,96,256]{3,2,1,0:T(8,128)(2,1)} %bitcast.8, bf16[4,4,96,256]{3,2,1,0:T(8,128)(2,1)} %bitcast.9, f32[1,256]{1,0:T(1,128)} %bitcast.10, f32[1,256]{1,0:T(1,128)} %bitcast.11, bf16[256,4096]{1,0:T(8,128)(2,1)} %wu_in.1, bf16[4096,256]{1,0:T(8,128)(2,1)} %wd_in.1, f32[1,256]{1,0:T(1,128)} %bitcast.12, ...), custom_call_target="tpu_custom_call" | custom-call | tf_op jit(solution)/shard_map/pallas_call | solution.py:480
  104.7 2.1 %copy.10 = bf16[1536,256]{1,0:T(8,128)(2,1)} copy(bf16[1536,256]{1,0:T(8,128)(2,1)} %bitcast.7) | data formatting | bytes 1572864

commit v4 on v3

--- a/solution.py
+++ b/solution.py
@@ -24,8 +24,8 @@
     car, bra, gi, bi, wu_in, wd_in, go, bo, out,
     cbuf, bbuf, nloc, nb, wu, wd, hid, pf, pb, opp_p, opp_m, sum_p, sum_m,
     from_m, from_p, rsum, tosend, torecv, mo, mob, obuf,
-    sx_s, sx_r, sz_s, sz_r, tx_s, tx_r, tz_s, tz_r, totals,
-    send_sem, recv_sem, local_sem,
+    sx_s, sx_r, tx_s, tx_r, totals, picked,
+    send_sem, recv_sem, local_sem, hello,
 ):
     r = lax.axis_index("ra")
     y = lax.axis_index("cb")
@@ -44,6 +44,12 @@
 
     def at_y(d):
         return (r, turn(y, d), c)
+
+    def at_zx(d):
+        return (turn(z, d // 4) * 4 + turn(x, d % 4), y, c)
+
+    def at_zy(d):
+        return (turn(z, d // 4) * 4 + x, turn(y, d % 4), c)
 
     partner = (r, y, 1 - c)
     remote = []
@@ -124,9 +130,13 @@
     load_wd = fetch(wd_in.at[rows(x * FS + c * 512, 512, 512), :], wd.at[x, wd_half, :])
 
     barrier = pltpu.get_barrier_semaphore()
-    friends = [dev(d) for dev in (at_x, at_z, at_y) for d in (1, 2, 3)] + [partner]
+    friends = [at_zx(d) for d in range(1, 16)] + [at_zy(d) for d in range(1, 16) if d % 4]
     for device in friends:
         pl.semaphore_signal(barrier, inc=1, device_id=device, device_id_type=MESH)
+
+    @pl.when(c == 0)
+    def _():
+        pl.semaphore_signal(barrier, inc=1, device_id=partner, device_id_type=MESH)
 
     def mixed_of(i):
         return residual_scale * cbuf[i].astype(F32) + bbuf[i].astype(F32)
@@ -144,21 +154,37 @@
         var = spread[:, 1:2] / D - mean * mean
         return mean, lax.rsqrt(var + norm_eps)
 
-    def exchange_start(buf, own, got, dev):
+    def exchange_start(buf, own, got, dev, n):
         buf[...] = own
         on = channel()
-        for d in (1, 2, 3):
+        for d in range(1, n):
             send(buf, got.at[d - 1], dev(d), on)
         return on
 
     def exchange_end(on, buf, got):
         expect(on, got)
-        return buf[...] + got[0] + got[1] + got[2]
+        return sum((got[d] for d in range(got.shape[0])), buf[...])
 
     d2d = (channel(), channel())
 
+    held = []
+
     def share(zz, xx, f):
-        send(wblk(zz, xx, f), wblk(zz, xx, f), partner, d2d[f])
+        if held is None:
+            send(wblk(zz, xx, f), wblk(zz, xx, f), partner, d2d[f])
+        else:
+            held.append((zz, xx, f))
+
+    def share_held():
+        nonlocal held
+
+        @pl.when(c == 0)
+        def _():
+            pl.semaphore_wait(hello, 1)
+
+        ready, held = held, None
+        for one in ready:
+            share(*one)
 
     def shared(f):
         expect(d2d[f], wu.at[pl.ds(0, D // 2), pl.ds(f * 512, 512)])
@@ -194,19 +220,20 @@
     mixed_in = jnp.concatenate([mixed_of(i) for i in range(4)], axis=0)
     own_sums = sums_of(mixed_in)
     load_wu.wait()
-    pl.semaphore_wait(barrier, len(friends))
-
-    stat = exchange_start(sx_s, own_sums, sx_r, at_x)
+    pl.semaphore_wait(barrier, len(friends) + c)
+
+    @pl.when(c == 1)
+    def _():
+        pl.semaphore_signal(hello, inc=1, device_id=partner, device_id_type=MESH)
+
+    stat = exchange_start(sx_s, own_sums, sx_r, at_zx, 16)
     w_start(0, 0)
     for d in (1, 3, 2):
         wu_send(d, 0)
     w_start(0, 1)
     wu_send(1, 1)
     wu_send(3, 1)
-    part = exchange_end(stat, sx_s, sx_r)
-    stat = exchange_start(sz_s, part, sz_r, at_z)
-    w_start(1, 0)
-    mean, scale = columns_of(exchange_end(stat, sz_s, sz_r))
+    mean, scale = columns_of(exchange_end(stat, sx_s, sx_r))
     normed = (
         (jnp.concatenate([mixed_of(i) for i in range(4)], axis=0) - mean) * scale * gi[...]
         + bi[...]
@@ -220,6 +247,7 @@
     for d in (1, 3, 2):
         send(nloc.at[turn(z, d)], mine, at_z(d), nsend)
     nb[rows(y * Q, Q, 32), rows(ncol, W, W)] = nloc[z]
+    w_start(1, 0)
     w_start(3, 0)
     w_forward(0, 0)
     expect(nsend, nloc.at[pl.ds(0, 3)])
@@ -258,6 +286,7 @@
     a1.forward()
     n_start(1)
     n_start(3)
+    share_held()
     wu_send(2, 1)
     w_start(1, 1)
     w_forward(3, 0)
@@ -295,7 +324,10 @@
 
     def up(n):
         cols = slice(n * 256, (n + 1) * 256)
-        pre = jnp.dot(nb[...], wu[:, cols], preferred_element_type=F32)
+        pre = sum(
+            jnp.dot(nb[:, i : i + 1024], wu[i : i + 1024, cols], preferred_element_type=F32)
+            for i in range(0, D, 1024)
+        )
         hid[z, :, cols] = jnp.square(jnp.maximum(pre, 0.0)).astype(BF)
 
         def hblk(i, half):
@@ -437,31 +469,34 @@
     fourth(3)
     pad = jnp.zeros((32, W), F32)
     mixed_out = jnp.concatenate([a for i in range(4) for a in (mo[i], pad)], axis=0)
-    stat = exchange_start(tx_s, sums_of(mixed_out), tx_r, at_x)
+    stat = exchange_start(tx_s, sums_of(mixed_out), tx_r, at_x, 4)
     last = channel()
     for d in (1, 3, 2):
         send(mob.at[y, 3], mob.at[y, 3], at_y(d), last)
-    part = exchange_end(stat, tx_s, tx_r)
-    stat = exchange_start(tz_s, part, tz_r, at_z)
     ring.forward()
+    totals[0] = exchange_end(stat, tx_s, tx_r)
+    stat = channel()
+    for d in range(1, 16):
+        send(totals.at[0], totals.at[d], at_zy(d), stat)
     ring.finish()
     expect(last, mob.at[pl.ds(0, 3), 3])
-    totals[y] = exchange_end(stat, tz_s, tz_r)
-    stat = channel()
-    for d in (1, 3, 2):
-        send(totals.at[y], totals.at[y], at_y(d), stat)
-
-    def finish(yy):
+    expect(stat, totals.at[pl.ds(1, 15)])
+    stacked = []
+    for dy in range(4):
+        sums = totals[dy] + totals[4 + dy] + totals[8 + dy] + totals[12 + dy]
+        picked[dy] = sums
         for k in range(4):
-            mean, scale = columns_of(totals[yy, :, rows(groups[k] * 128, 128, 128)])
-            block = (mob[yy, k].astype(F32) - mean[0:Q]) * scale[0:Q] * go[...] + bo[...]
-            obuf[yy, k] = block.astype(BF)
+            stacked.append(picked[dy, :, rows(groups[k] * 128, 128, 128)])
+    columns = jnp.transpose(jnp.concatenate(stacked, axis=0))[0:Q]
+    for dy in range(4):
+        yy = turn(y, -dy)
+        for k in range(4):
+            at = (dy * 4 + k) * 8
+            mean = columns[:, at : at + 1] / D
+            var = columns[:, at + 1 : at + 2] / D - mean * mean
+            block = (mob[yy, k].astype(F32) - mean) * lax.rsqrt(var + norm_eps)
+            obuf[yy, k] = (block * go[...] + bo[...]).astype(BF)
             fetch(obuf.at[yy, k], out.at[groups[k], yy], 4)
-
-    finish(y)
-    expect(stat, totals.at[pl.ds(0, 3)])
-    for d in (1, 3, 2):
-        finish(turn(y, -d))
     assert len(used) == N_RECV, len(used)
     for copy in remote[-N_SEND:]:
         copy.wait_send()
@@ -469,7 +504,7 @@
 
 
 N_SEND = 64
-N_RECV = 126
+N_RECV = 124
 N_LOCAL = 5
 
 
@@ -490,12 +525,12 @@
             V((4, 2, 4, 48, W), BF), V((4, 2, 4, 48, W), BF),
             V((4, 2, 4, 48, W), F32), V((4, 2, 4, 48, W), BF), V((4, 2, 3, 48, W), BF),
             V((4, Q, W), F32), V((4, 4, Q, W), BF), V((4, 4, Q, W), BF),
-            *[V(shape, F32) for shape in ((8, G), (3, 8, G)) * 2],
-            *[V(shape, F32) for shape in ((8, 512), (3, 8, 512)) * 2],
-            V((4, 8, 512), F32),
+            V((8, G), F32), V((15, 8, G), F32),
+            V((8, 512), F32), V((3, 8, 512), F32), V((16, 8, 512), F32), V((4, 8, 512), F32),
             pltpu.SemaphoreType.DMA((N_SEND,)),
             pltpu.SemaphoreType.DMA((N_RECV,)),
             pltpu.SemaphoreType.DMA((N_LOCAL,)),
+            pltpu.SemaphoreType.REGULAR,
         ],
         compiler_params=pltpu.CompilerParams(
             collective_id=0, has_side_effects=True, vmem_limit_bytes=60 * 1024 * 1024

time: 107 us -> 108 us (level)
  no operation moved by 1% of the time
where the time goes in v4:
time: 108 us
  Pallas kernels  106 us (98%)
  local copies, waits for them, and re-layouts  2.06 us (2%)
    pallas_call x1, Pallas kernels, per_device(): pl.pallas_call(kernel, out_shape=jax.ShapeDtypeStruct((4, 4, Q, W), BF),...  106 us

profile of v4, /device:TPU:0, one launch (start us, length us, event | category | flops | bytes accessed | tf_op | source)
XLA Modules:
  0.0 107.8 jit_solution(14128142956270018576)
XLA Ops:
  0.0 105.7 %shard_map.82 = bf16[4,4,96,256]{3,2,1,0:T(8,128)(2,1)} custom-call(bf16[4,4,96,256]{3,2,1,0:T(8,128)(2,1)} %bitcast.8, bf16[4,4,96,256]{3,2,1,0:T(8,128)(2,1)} %bitcast.9, f32[1,256]{1,0:T(1,128)} %bitcast.10, f32[1,256]{1,0:T(1,128)} %bitcast.11, bf16[256,4096]{1,0:T(8,128)(2,1)} %wu_in.1, bf16[4096,256]{1,0:T(8,128)(2,1)} %wd_in.1, f32[1,256]{1,0:T(1,128)} %bitcast.12, ...), custom_call_target="tpu_custom_call" | custom-call | tf_op jit(solution)/shard_map/pallas_call | solution.py:515
  105.7 2.1 %copy.10 = bf16[1536,256]{1,0:T(8,128)(2,1)} copy(bf16[1536,256]{1,0:T(8,128)(2,1)} %bitcast.7) | data formatting | bytes 1572864

commit v5 on v4

--- a/solution.py
+++ b/solution.py
@@ -24,7 +24,7 @@
     car, bra, gi, bi, wu_in, wd_in, go, bo, out,
     cbuf, bbuf, nloc, nb, wu, wd, hid, pf, pb, opp_p, opp_m, sum_p, sum_m,
     from_m, from_p, rsum, tosend, torecv, mo, mob, obuf,
-    sx_s, sx_r, tx_s, tx_r, totals, picked,
+    sx_s, sx_r, tx_s, tx_r, totals,
     send_sem, recv_sem, local_sem, hello,
 ):
     r = lax.axis_index("ra")
@@ -141,17 +141,23 @@
     def mixed_of(i):
         return residual_scale * cbuf[i].astype(F32) + bbuf[i].astype(F32)
 
-    def sums_of(mixed):
-        total = jnp.sum(mixed, axis=1, keepdims=True)
-        square = jnp.sum(mixed * mixed, axis=1, keepdims=True)
-        lane = lax.broadcasted_iota(jnp.int32, (mixed.shape[0], 128), 1)
-        return jnp.transpose(jnp.where(lane == 0, total, square))[0:8]
+    def sums_of(groups):
+        lane = lax.broadcasted_iota(jnp.int32, (128, 128), 1)
+        packed = jnp.zeros((128, 128), F32)
+        pad = jnp.zeros((32, 1), F32)
+        for g, mixed in enumerate(groups):
+            total = jnp.sum(mixed, axis=1, keepdims=True)
+            square = jnp.sum(mixed * mixed, axis=1, keepdims=True)
+            packed = jnp.where(lane == g, jnp.concatenate([total, pad], axis=0), packed)
+            packed = jnp.where(lane == 4 + g, jnp.concatenate([square, pad], axis=0), packed)
+        return jnp.transpose(packed)[0:8]
 
     def columns_of(sums):
-        row = lax.broadcasted_iota(jnp.int32, (128, sums.shape[1]), 0)
-        spread = jnp.transpose(jnp.where(row == 0, sums[0:1], sums[1:2]))
-        mean = spread[:, 0:1] / D
-        var = spread[:, 1:2] / D - mean * mean
+        return jnp.transpose(jnp.concatenate(sums + [sums[0]] * (16 - len(sums)), axis=0))[0:Q]
+
+    def moments(columns, at):
+        mean = columns[:, at : at + 1] / D
+        var = columns[:, at + 4 : at + 5] / D - mean * mean
         return mean, lax.rsqrt(var + norm_eps)
 
     def exchange_start(buf, own, got, dev, n):
@@ -217,8 +223,7 @@
 
     load_c.wait()
     load_b.wait()
-    mixed_in = jnp.concatenate([mixed_of(i) for i in range(4)], axis=0)
-    own_sums = sums_of(mixed_in)
+    own_sums = sums_of([mixed_of(i) for i in range(4)])
     load_wu.wait()
     pl.semaphore_wait(barrier, len(friends) + c)
 
@@ -233,13 +238,10 @@
     w_start(0, 1)
     wu_send(1, 1)
     wu_send(3, 1)
-    mean, scale = columns_of(exchange_end(stat, sx_s, sx_r))
-    normed = (
-        (jnp.concatenate([mixed_of(i) for i in range(4)], axis=0) - mean) * scale * gi[...]
-        + bi[...]
-    ).astype(BF)
+    columns = columns_of([exchange_end(stat, sx_s, sx_r)])
     for i in range(4):
-        nloc[i] = normed[i * Q : (i + 1) * Q]
+        mean, scale = moments(columns, i)
+        nloc[i] = ((mixed_of(i) - mean) * scale * gi[...] + bi[...]).astype(BF)
 
     ncol = (lax.div(z, 2) * 4 + x) * 512 + lax.rem(z, 2) * 256
     mine = nb.at[rows(y * Q, Q, 32), rows(ncol, W, W)]
@@ -280,33 +282,29 @@
     a1.start()
     b1.start()
     n_start(0)
+    wu_send(2, 1)
     w_start(2, 0)
+    w_forward(0, 1)
+    w_start(3, 1)
     w_forward(1, 0)
     b1.forward()
     a1.forward()
     n_start(1)
     n_start(3)
-    share_held()
-    wu_send(2, 1)
     w_start(1, 1)
     w_forward(3, 0)
-    w_forward(0, 1)
+    share_held()
     n_forward(0)
     b1.finish()
     a1.finish()
     n_start(2)
-    w_start(3, 1)
+    w_start(2, 1)
     w_forward(2, 0)
-    for u in (0, 1, 3):
-        w_finish(u, 0)
     n_forward(1)
-    w_forward(1, 1)
-    w_start(2, 1)
-    w_finish(2, 0)
-    w_finish(0, 1)
     n_forward(3)
     w_forward(3, 1)
     n_forward(2)
+    w_forward(1, 1)
 
     wd_a2a, wshare = channel(), channel()
     for d in (1, 3, 2):
@@ -314,10 +312,12 @@
         part = wd_in.at[rows(to * FS + c * 512, 512, 512), :]
         send(part, wd.at[x, wd_half, :], at_x(d), wd_a2a)
     load_wd.wait()
-    w_forward(2, 1)
+    for u in range(4):
+        w_finish(u, 0)
     for pair in seconds:
         for ring in pair:
             ring.finish()
+    w_forward(2, 1)
     shared(0)
 
     hrings = []
@@ -340,7 +340,7 @@
         hrings.append(ring)
 
     up(0)
-    for u in (1, 3, 2):
+    for u in (0, 3, 1, 2):
         w_finish(u, 1)
     up(1)
     expect(wd_a2a, wd.at[pl.ds(0, 3), wd_half, :])
@@ -415,9 +415,10 @@
             part = slice(self.kind * 48, self.kind * 48 + 48)
             mixed = residual_scale * nloc[group, part].astype(F32) + branch
             mo[group, part] = mixed
-            mob[y, self.k, part] = mixed.astype(BF)
+            mob[y, places[self.k], part] = mixed.astype(BF)
 
     groups = [z, turn(z, -1), turn(z, 1), turn(z, 2)]
+    places = [1, 0, 2, 3]
     reduces = [(Reduce(k, 0), Reduce(k, 1)) for k in range(4)]
 
     def first(k):
@@ -449,11 +450,11 @@
     fourth(0)
     second_(1)
     second_(2)
-    third(1)
-    third(2)
     for ring in hrings:
         ring.finish()
     first(3)
+    third(1)
+    third(2)
     second_(3)
     fourth(1)
     fourth(2)
@@ -467,9 +468,7 @@
     ring = Ring(y, at_y, mblk)
     ring.start()
     fourth(3)
-    pad = jnp.zeros((32, W), F32)
-    mixed_out = jnp.concatenate([a for i in range(4) for a in (mo[i], pad)], axis=0)
-    stat = exchange_start(tx_s, sums_of(mixed_out), tx_r, at_x, 4)
+    stat = exchange_start(tx_s, sums_of([mo[i] for i in range(4)]), tx_r, at_x, 4)
     last = channel()
     for d in (1, 3, 2):
         send(mob.at[y, 3], mob.at[y, 3], at_y(d), last)
@@ -481,22 +480,14 @@
     ring.finish()
     expect(last, mob.at[pl.ds(0, 3), 3])
     expect(stat, totals.at[pl.ds(1, 15)])
-    stacked = []
-    for dy in range(4):
-        sums = totals[dy] + totals[4 + dy] + totals[8 + dy] + totals[12 + dy]
-        picked[dy] = sums
-        for k in range(4):
-            stacked.append(picked[dy, :, rows(groups[k] * 128, 128, 128)])
-    columns = jnp.transpose(jnp.concatenate(stacked, axis=0))[0:Q]
+    columns = columns_of([totals[i] + totals[4 + i] + totals[8 + i] + totals[12 + i] for i in range(4)])
     for dy in range(4):
         yy = turn(y, -dy)
-        for k in range(4):
-            at = (dy * 4 + k) * 8
-            mean = columns[:, at : at + 1] / D
-            var = columns[:, at + 1 : at + 2] / D - mean * mean
-            block = (mob[yy, k].astype(F32) - mean) * lax.rsqrt(var + norm_eps)
-            obuf[yy, k] = (block * go[...] + bo[...]).astype(BF)
-            fetch(obuf.at[yy, k], out.at[groups[k], yy], 4)
+        for g in range(4):
+            mean, scale = moments(columns, dy * 8 + g)
+            block = (mob[yy, turn(1 - z, g)].astype(F32) - mean) * scale
+            obuf[yy, g] = (block * go[...] + bo[...]).astype(BF)
+            fetch(obuf.at[yy, g], out.at[g, yy], 4)
     assert len(used) == N_RECV, len(used)
     for copy in remote[-N_SEND:]:
         copy.wait_send()
@@ -525,8 +516,8 @@
             V((4, 2, 4, 48, W), BF), V((4, 2, 4, 48, W), BF),
             V((4, 2, 4, 48, W), F32), V((4, 2, 4, 48, W), BF), V((4, 2, 3, 48, W), BF),
             V((4, Q, W), F32), V((4, 4, Q, W), BF), V((4, 4, Q, W), BF),
-            V((8, G), F32), V((15, 8, G), F32),
-            V((8, 512), F32), V((3, 8, 512), F32), V((16, 8, 512), F32), V((4, 8, 512), F32),
+            V((8, 128), F32), V((15, 8, 128), F32),
+            V((8, 128), F32), V((3, 8, 128), F32), V((16, 8, 128), F32),
             pltpu.SemaphoreType.DMA((N_SEND,)),
             pltpu.SemaphoreType.DMA((N_RECV,)),
             pltpu.SemaphoreType.DMA((N_LOCAL,)),

time: 108 us -> 101 us (0.935)
  Pallas kernels: 106 us -> 98.6 us
    pallas_call x1, Pallas kernels: 106 us -> 98.6 us  [per_device(): pl.pallas_call(kernel, out_shape=jax.ShapeDtypeStruct((4, 4, Q, W), BF),...]
where the time goes in v5:
time: 101 us
  Pallas kernels  98.6 us (98%)
  local copies, waits for them, and re-layouts  2.06 us (2%)
    pallas_call x1, Pallas kernels, per_device(): pl.pallas_call(kernel, out_shape=jax.ShapeDtypeStruct((4, 4, Q, W), BF),...  98.6 us
    unnamed x1, local copies, waits for them, and re-layouts  2.06 us

profile of v5, /device:TPU:0, one launch (start us, length us, event | category | flops | bytes accessed | tf_op | source)
XLA Modules:
  0.0 100.6 jit_solution(9315313583235369205)
XLA Ops:
  0.0 98.6 %shard_map.82 = bf16[4,4,96,256]{3,2,1,0:T(8,128)(2,1)} custom-call(bf16[4,4,96,256]{3,2,1,0:T(8,128)(2,1)} %bitcast.8, bf16[4,4,96,256]{3,2,1,0:T(8,128)(2,1)} %bitcast.9, f32[1,256]{1,0:T(1,128)} %bitcast.10, f32[1,256]{1,0:T(1,128)} %bitcast.11, bf16[256,4096]{1,0:T(8,128)(2,1)} %wu_in.1, bf16[4096,256]{1,0:T(8,128)(2,1)} %wd_in.1, f32[1,256]{1,0:T(1,128)} %bitcast.12, ...), custom_call_target="tpu_custom_call" | custom-call | tf_op jit(solution)/shard_map/pallas_call | solution.py:506
  98.6 2.1 %copy.10 = bf16[1536,256]{1,0:T(8,128)(2,1)} copy(bf16[1536,256]{1,0:T(8,128)(2,1)} %bitcast.7) | data formatting | bytes 1572864

commit v6 on v5

--- a/solution.py
+++ b/solution.py
@@ -23,9 +23,9 @@
 def kernel(
     car, bra, gi, bi, wu_in, wd_in, go, bo, out,
     cbuf, bbuf, nloc, nb, wu, wd, hid, pf, pb, opp_p, opp_m, sum_p, sum_m,
-    from_m, from_p, rsum, tosend, torecv, mo, mob, obuf,
+    from_m, from_p, direct, rsum, tosend, torecv, mo, mob, obuf,
     sx_s, sx_r, tx_s, tx_r, totals,
-    send_sem, recv_sem, local_sem, hello,
+    send_sem, recv_sem, local_sem, hello, plane_x, plane_y,
 ):
     r = lax.axis_index("ra")
     y = lax.axis_index("cb")
@@ -130,7 +130,7 @@
     load_wd = fetch(wd_in.at[rows(x * FS + c * 512, 512, 512), :], wd.at[x, wd_half, :])
 
     barrier = pltpu.get_barrier_semaphore()
-    friends = [at_zx(d) for d in range(1, 16)] + [at_zy(d) for d in range(1, 16) if d % 4]
+    friends = [dev(d) for dev in (at_x, at_z, at_y) for d in (1, 2, 3)]
     for device in friends:
         pl.semaphore_signal(barrier, inc=1, device_id=device, device_id_type=MESH)
 
@@ -231,13 +231,17 @@
     def _():
         pl.semaphore_signal(hello, inc=1, device_id=partner, device_id_type=MESH)
 
+    for d in (1, 2, 3):
+        pl.semaphore_signal(plane_x, inc=1, device_id=at_x(d), device_id_type=MESH)
+        pl.semaphore_signal(plane_y, inc=1, device_id=at_y(d), device_id_type=MESH)
+    pl.semaphore_wait(plane_x, 3)
     stat = exchange_start(sx_s, own_sums, sx_r, at_zx, 16)
     w_start(0, 0)
     for d in (1, 3, 2):
         wu_send(d, 0)
     w_start(0, 1)
-    wu_send(1, 1)
-    wu_send(3, 1)
+    for d in (1, 3, 2):
+        wu_send(d, 1)
     columns = columns_of([exchange_end(stat, sx_s, sx_r)])
     for i in range(4):
         mean, scale = moments(columns, i)
@@ -246,12 +250,12 @@
     ncol = (lax.div(z, 2) * 4 + x) * 512 + lax.rem(z, 2) * 256
     mine = nb.at[rows(y * Q, Q, 32), rows(ncol, W, W)]
     nsend = channel()
-    for d in (1, 3, 2):
+    for d in (2, 1, 3):
         send(nloc.at[turn(z, d)], mine, at_z(d), nsend)
     nb[rows(y * Q, Q, 32), rows(ncol, W, W)] = nloc[z]
+    w_forward(0, 0)
     w_start(1, 0)
     w_start(3, 0)
-    w_forward(0, 0)
     expect(nsend, nloc.at[pl.ds(0, 3)])
 
     def nblk(h, xx, yy, part):
@@ -282,27 +286,25 @@
     a1.start()
     b1.start()
     n_start(0)
-    wu_send(2, 1)
     w_start(2, 0)
-    w_forward(0, 1)
-    w_start(3, 1)
-    w_forward(1, 0)
     b1.forward()
     a1.forward()
     n_start(1)
     n_start(3)
-    w_start(1, 1)
-    w_forward(3, 0)
+    w_forward(1, 0)
     share_held()
     n_forward(0)
+    w_forward(3, 0)
     b1.finish()
     a1.finish()
     n_start(2)
+    w_start(1, 1)
+    w_forward(2, 0)
+    w_start(3, 1)
     w_start(2, 1)
-    w_forward(2, 0)
+    w_forward(0, 1)
     n_forward(1)
     n_forward(3)
-    w_forward(3, 1)
     n_forward(2)
     w_forward(1, 1)
 
@@ -312,15 +314,15 @@
         part = wd_in.at[rows(to * FS + c * 512, 512, 512), :]
         send(part, wd.at[x, wd_half, :], at_x(d), wd_a2a)
     load_wd.wait()
-    for u in range(4):
+    for u in (0, 1, 3, 2):
         w_finish(u, 0)
     for pair in seconds:
         for ring in pair:
             ring.finish()
-    w_forward(2, 1)
+    w_forward(3, 1)
     shared(0)
 
-    hrings = []
+    hsent = []
 
     def up(n):
         cols = slice(n * 256, (n + 1) * 256)
@@ -328,156 +330,195 @@
             jnp.dot(nb[:, i : i + 1024], wu[i : i + 1024, cols], preferred_element_type=F32)
             for i in range(0, D, 1024)
         )
-        hid[z, :, cols] = jnp.square(jnp.maximum(pre, 0.0)).astype(BF)
-
-        def hblk(i, half):
-            if half is None:
-                return hid.at[i, :, pl.ds(n * 256, 256)]
-            return hid.at[i, pl.ds(half * 192, 192), pl.ds(n * 256, 256)]
-
-        ring = Ring(z, at_z, hblk)
-        ring.start()
-        hrings.append(ring)
+        hidden = jnp.square(jnp.maximum(pre, 0.0)).astype(BF)
+        for i in range(4):
+            hid[z, i, :, cols] = hidden[i * Q : (i + 1) * Q]
+
+    def h_start(n):
+        mine = hid.at[z, :, :, pl.ds(n * 256, 256)]
+        hsent.append((send(mine, mine, at_z(1)), send(mine, mine, at_z(-1))))
+
+    hon = (channel(), channel())
+
+    def h_forward(n, late):
+        for i, copy in enumerate(hsent[n]):
+            if not late:
+                copy.wait_recv()
+            group = turn(z, 2 * i - 1)
+            part = hid.at[group, pl.ds(2 * i, 2), pl.ds(48 * late, 48), pl.ds(n * 256, 256)]
+            send(part, part, at_z(1 - 2 * i), hon[late])
 
     up(0)
-    for u in (0, 3, 1, 2):
+    w_forward(2, 1)
+    h_start(0)
+    up(1)
+    h_start(1)
+    for u in (0, 1, 3, 2):
         w_finish(u, 1)
-    up(1)
+    shared(1)
+    up(2)
+    h_start(2)
     expect(wd_a2a, wd.at[pl.ds(0, 3), wd_half, :])
     send(wd.at[:, wd_half, :], wd.at[:, wd_half, :], partner, wshare)
-    shared(1)
-    up(2)
     up(3)
+    h_start(3)
     expect(wshare, wd.at[:, wd_half, :])
 
-    def down(k, group):
+    def down(k, group, at):
+        size = 4 * at.size
+        lhs = hid[group, :, at].reshape(size, FS)
         for j in range(4):
-            part = jnp.dot(hid[group], wd[j], preferred_element_type=F32)
-            for i in range(4):
-                pf[k, j, i] = part[i * Q : (i + 1) * Q]
-                pb[k, j, i] = part[i * Q : (i + 1) * Q].astype(BF)
+            part = jnp.dot(lhs, wd[j], preferred_element_type=F32).reshape(4, at.size, W)
+            for kind in range(2):
+                lanes = slice(kind * 128, kind * 128 + 128)
+                pf[k, kind, j, :, at] = part[:, :, lanes]
+                pb[k, kind, j, :, at] = part[:, :, lanes].astype(BF)
 
     class Reduce:
-        def __init__(self, k, kind):
-            self.at = (k, kind)
-            self.k = k
-            self.kind = kind
+        def __init__(self, k, kind, at):
+            self.k, self.kind, self.rows = k, kind, at
             self.pos, self.dev = ((y, at_y), (x, at_x))[kind]
             self.pos2, self.dev2 = ((x, at_x), (y, at_y))[kind]
 
         def item(self, to, first, count):
-            if self.kind == 0:
-                return (self.k, pl.ds(first, count), to, pl.ds(0, 48), slice(None))
-            return (self.k, to, pl.ds(first, count), pl.ds(48, 48), slice(None))
+            where = (pl.ds(first, count), to) if self.kind == 0 else (to, pl.ds(first, count))
+            return (self.k, self.kind, *where, self.rows)
+
+        def of(self, ref, *where):
+            return (ref.at[(self.k, self.kind, *where, self.rows)])
 
         def first(self):
+            self.on_m, self.on_2 = channel(), channel()
+            if self.k == 3:
+                for d in (2, 1, 3):
+                    part = pb.at[self.item(turn(self.pos, d), 0, 4)]
+                    send(part, direct.at[self.kind, d - 1, :, self.rows], self.dev(d), self.on_m)
+                return
+            self.on_p = channel()
             far, p, m = turn(self.pos, 2), turn(self.pos, 1), turn(self.pos, -1)
             self.p, self.m = p, m
-            self.op = send(pb.at[self.item(far, 0, 2)], opp_p.at[self.at], self.dev(1))
-            self.om = send(pb.at[self.item(far, 2, 2)], opp_m.at[self.at], self.dev(-1))
             low, high = pl.ds(0, 2), pl.ds(2, 2)
-            self.on_m, self.on_p, self.on_2 = channel(), channel(), channel()
-            send(
-                pb.at[self.item(p, 2, 2)], from_m.at[(*self.at, high)], self.dev(1), self.on_m
-            )
-            send(
-                pb.at[self.item(m, 0, 2)], from_p.at[(*self.at, low)], self.dev(-1), self.on_p
-            )
+            self.op = send(pb.at[self.item(far, 0, 2)], self.of(opp_p, slice(None)), self.dev(1))
+            self.om = send(pb.at[self.item(far, 2, 2)], self.of(opp_m, slice(None)), self.dev(-1))
+            send(pb.at[self.item(p, 2, 2)], self.of(from_m, high), self.dev(1), self.on_m)
+            send(pb.at[self.item(m, 0, 2)], self.of(from_p, low), self.dev(-1), self.on_p)
 
         def second(self):
-            low, high = pl.ds(0, 2), pl.ds(2, 2)
+            at = (self.k, self.kind)
             self.op.wait_recv()
-            sum_p[self.at] = (pf[self.item(self.p, 0, 2)] + opp_p[self.at].astype(F32)).astype(BF)
-            send(sum_p.at[self.at], from_m.at[(*self.at, low)], self.dev(1), self.on_m)
+            sum_p[at] = (pf[self.item(self.p, 0, 2)] + opp_p[at].astype(F32)).astype(BF)
+            send(sum_p.at[at], self.of(from_m, pl.ds(0, 2)), self.dev(1), self.on_m)
             self.om.wait_recv()
-            sum_m[self.at] = (pf[self.item(self.m, 2, 2)] + opp_m[self.at].astype(F32)).astype(BF)
-            send(sum_m.at[self.at], from_p.at[(*self.at, high)], self.dev(-1), self.on_p)
+            sum_m[at] = (pf[self.item(self.m, 2, 2)] + opp_m[at].astype(F32)).astype(BF)
+            send(sum_m.at[at], self.of(from_p, pl.ds(2, 2)), self.dev(-1), self.on_p)
 
         def third(self):
-            expect(self.on_m, from_m.at[self.at])
-            expect(self.on_p, from_p.at[self.at])
-            total = (
-                pf[self.item(self.pos, 0, 4)]
-                + from_m[self.at].astype(F32)
-                + from_p[self.at].astype(F32)
-            )
-            rsum[self.at] = total
-            tosend[self.at] = total.astype(BF)
+            total = pf[self.item(self.pos, 0, 4)]
+            if self.k == 3:
+                expect(self.on_m, direct.at[self.kind, :, :, self.rows])
+                for d in range(3):
+                    total = total + direct[self.kind, d, :, self.rows].astype(F32)
+            else:
+                at = (self.k, self.kind)
+                expect(self.on_m, from_m.at[at])
+                expect(self.on_p, from_p.at[at])
+                total = total + from_m[at].astype(F32) + from_p[at].astype(F32)
+            rsum[self.k, self.kind, :, self.rows] = total
+            tosend[self.k, self.kind, :, self.rows] = total.astype(BF)
             for d in (1, 3, 2):
                 to = turn(self.pos2, d)
-                send(tosend.at[(*self.at, to)], torecv.at[(*self.at, d - 1)], self.dev2(d), self.on_2)
+                send(self.of(tosend, to), self.of(torecv, d - 1), self.dev2(d), self.on_2)
 
         def fourth(self, group):
-            expect(self.on_2, torecv.at[self.at])
-            branch = rsum[(*self.at, self.pos2)]
+            expect(self.on_2, self.of(torecv, slice(None)))
+            branch = rsum[self.k, self.kind, self.pos2, self.rows]
             for d in range(3):
-                branch = branch + torecv[(*self.at, d)].astype(F32)
-            part = slice(self.kind * 48, self.kind * 48 + 48)
-            mixed = residual_scale * nloc[group, part].astype(F32) + branch
-            mo[group, part] = mixed
-            mob[y, places[self.k], part] = mixed.astype(BF)
+                branch = branch + torecv[self.k, self.kind, d, self.rows].astype(F32)
+            lanes = slice(self.kind * 128, self.kind * 128 + 128)
+            mixed = residual_scale * nloc[group, self.rows, lanes].astype(F32) + branch
+            mo[group, self.rows, lanes] = mixed
+            mob[y, places[self.k], self.rows, lanes] = mixed.astype(BF)
 
     groups = [z, turn(z, -1), turn(z, 1), turn(z, 2)]
     places = [1, 0, 2, 3]
-    reduces = [(Reduce(k, 0), Reduce(k, 1)) for k in range(4)]
-
-    def first(k):
-        down(k, groups[k])
-        for one in reduces[k]:
+    batches = [(0, pl.ds(0, Q)), (1, pl.ds(0, Q)), (2, pl.ds(0, Q)), (3, pl.ds(0, 48)), (3, pl.ds(48, 48))]
+    reduces = [(Reduce(k, 0, at), Reduce(k, 1, at)) for k, at in batches]
+
+    def first(b):
+        k, at = batches[b]
+        down(k, groups[k], at)
+        for one in reduces[b]:
             one.first()
 
-    def second_(k):
-        for one in reduces[k]:
+    def second_(b):
+        for one in reduces[b]:
             one.second()
 
-    def third(k):
-        for one in reduces[k]:
+    def third(b):
+        for one in reduces[b]:
             one.third()
 
-    def fourth(k):
-        for one in reduces[k]:
-            one.fourth(groups[k])
+    def fourth(b):
+        for one in reduces[b]:
+            one.fourth(groups[batches[b][0]])
+
+    def h_finish(late):
+        expect(hon[late], hid.at[0, :, pl.ds(0, 48), :])
 
     first(0)
-    hrings[0].forward()
-    hrings[1].forward()
+    h_forward(0, 0)
+    h_forward(1, 0)
     second_(0)
-    hrings[2].forward()
+    h_forward(2, 0)
     third(0)
-    hrings[3].forward()
+    h_forward(3, 0)
+    for n in range(4):
+        h_forward(n, 1)
+    def gather(place):
+        def mblk(i, half):
+            if half is None:
+                return mob.at[i, place]
+            return mob.at[i, place, pl.ds(half * 48, 48)]
+
+        ring = Ring(y, at_y, mblk)
+        ring.start()
+        return ring
+
     first(1)
     first(2)
     fourth(0)
+    gathers = [gather(places[0])]
     second_(1)
     second_(2)
-    for ring in hrings:
-        ring.finish()
+    h_finish(0)
     first(3)
     third(1)
+    gathers[0].forward()
+    h_finish(1)
+    first(4)
     third(2)
-    second_(3)
+    third(3)
     fourth(1)
+    gathers.append(gather(places[1]))
+    third(4)
     fourth(2)
-    third(3)
-
-    def mblk(i, half):
-        if half is None:
-            return mob.at[i, pl.ds(0, 3)]
-        return mob.at[i, pl.ds(0, 3), pl.ds(half * 48, 48)]
-
-    ring = Ring(y, at_y, mblk)
-    ring.start()
+    gathers.append(gather(places[2]))
     fourth(3)
+    fourth(4)
+
     stat = exchange_start(tx_s, sums_of([mo[i] for i in range(4)]), tx_r, at_x, 4)
     last = channel()
     for d in (1, 3, 2):
         send(mob.at[y, 3], mob.at[y, 3], at_y(d), last)
-    ring.forward()
     totals[0] = exchange_end(stat, tx_s, tx_r)
     stat = channel()
+    pl.semaphore_wait(plane_y, 3)
     for d in range(1, 16):
         send(totals.at[0], totals.at[d], at_zy(d), stat)
-    ring.finish()
+    gathers[1].forward()
+    gathers[2].forward()
+    for ring in gathers:
+        ring.finish()
     expect(last, mob.at[pl.ds(0, 3), 3])
     expect(stat, totals.at[pl.ds(1, 15)])
     columns = columns_of([totals[i] + totals[4 + i] + totals[8 + i] + totals[12 + i] for i in range(4)])
@@ -495,7 +536,7 @@
 
 
 N_SEND = 64
-N_RECV = 124
+N_RECV = 126
 N_LOCAL = 5
 
 
@@ -510,18 +551,18 @@
         out_specs=any_spec,
         scratch_shapes=[
             V((4, Q, W), BF), V((4, Q, W), BF), V((4, Q, W), BF),
-            V((G, D), BF), V((D, FS), BF), V((4, FS, W), BF), V((4, G, FS), BF),
-            V((4, 4, 4, Q, W), F32), V((4, 4, 4, Q, W), BF),
-            *[V((4, 2, 2, 48, W), BF) for _ in range(4)],
-            V((4, 2, 4, 48, W), BF), V((4, 2, 4, 48, W), BF),
-            V((4, 2, 4, 48, W), F32), V((4, 2, 4, 48, W), BF), V((4, 2, 3, 48, W), BF),
+            V((G, D), BF), V((D, FS), BF), V((4, FS, W), BF), V((4, 4, Q, FS), BF),
+            V((4, 2, 4, 4, Q, 128), F32), V((4, 2, 4, 4, Q, 128), BF),
+            *[V((3, 2, 2, Q, 128), BF) for _ in range(4)],
+            V((3, 2, 4, Q, 128), BF), V((3, 2, 4, Q, 128), BF), V((2, 3, 4, Q, 128), BF),
+            V((4, 2, 4, Q, 128), F32), V((4, 2, 4, Q, 128), BF), V((4, 2, 3, Q, 128), BF),
             V((4, Q, W), F32), V((4, 4, Q, W), BF), V((4, 4, Q, W), BF),
             V((8, 128), F32), V((15, 8, 128), F32),
             V((8, 128), F32), V((3, 8, 128), F32), V((16, 8, 128), F32),
             pltpu.SemaphoreType.DMA((N_SEND,)),
             pltpu.SemaphoreType.DMA((N_RECV,)),
             pltpu.SemaphoreType.DMA((N_LOCAL,)),
-            pltpu.SemaphoreType.REGULAR,
+            *[pltpu.SemaphoreType.REGULAR] * 3,
         ],
         compiler_params=pltpu.CompilerParams(
             collective_id=0, has_side_effects=True, vmem_limit_bytes=60 * 1024 * 1024

time: 101 us -> 99.9 us (0.989)
  no operation moved by 1% of the time
where the time goes in v6:
time: 99.9 us; the launch traced here: 99.7 us
  Pallas kernels  97.7 us (98%)
  local copies, waits for them, and re-layouts  2.06 us (2%)
    pallas_call x1, Pallas kernels, per_device(): pl.pallas_call(kernel, out_shape=jax.ShapeDtypeStruct((4, 4, Q, W), BF),...  97.7 us
    unnamed x1, local copies, waits for them, and re-layouts  2.06 us

profile of v6, /device:TPU:0, one launch (start us, length us, event | category | flops | bytes accessed | tf_op | source)
XLA Modules:
  0.0 99.7 jit_solution(16891727481734532232)
XLA Ops:
  0.0 97.7 %shard_map.82 = bf16[4,4,96,256]{3,2,1,0:T(8,128)(2,1)} custom-call(bf16[4,4,96,256]{3,2,1,0:T(8,128)(2,1)} %bitcast.8, bf16[4,4,96,256]{3,2,1,0:T(8,128)(2,1)} %bitcast.9, f32[1,256]{1,0:T(1,128)} %bitcast.10, f32[1,256]{1,0:T(1,128)} %bitcast.11, bf16[256,4096]{1,0:T(8,128)(2,1)} %wu_in.1, bf16[4096,256]{1,0:T(8,128)(2,1)} %wd_in.1, f32[1,256]{1,0:T(1,128)} %bitcast.12, ...), custom_call_target="tpu_custom_call" | custom-call | tf_op jit(solution)/shard_map/pallas_call | solution.py:547
  97.7 2.1 %copy.10 = bf16[1536,256]{1,0:T(8,128)(2,1)} copy(bf16[1536,256]{1,0:T(8,128)(2,1)} %bitcast.7) | data formatting | bytes 1572864

commit v7 on v6

--- a/solution.py
+++ b/solution.py
@@ -87,22 +87,21 @@
         return copy
 
     class Ring:
-        def __init__(self, pos, dev, blk):
-            self.pos, self.dev, self.blk = pos, dev, blk
+        def __init__(self, pos, dev, both, blk):
+            self.pos, self.dev, self.both, self.blk = pos, dev, both, blk
 
         def start(self):
+            self.to = channel()
             mine = self.blk(self.pos, None)
-            self.p = send(mine, mine, self.dev(1))
-            self.m = send(mine, mine, self.dev(-1))
+            send(mine, mine, self.dev(1), self.to)
+            send(mine, mine, self.dev(-1), self.to)
 
         def forward(self):
             self.on = channel()
-            self.p.wait_recv()
-            half = self.blk(turn(self.pos, -1), 0)
-            send(half, half, self.dev(1), self.on)
-            self.m.wait_recv()
-            half = self.blk(turn(self.pos, 1), 1)
-            send(half, half, self.dev(-1), self.on)
+            expect(self.to, self.both)
+            for i in range(2):
+                half = self.blk(turn(self.pos, 2 * i - 1), i)
+                send(half, half, self.dev(1 - 2 * i), self.on)
 
         def finish(self):
             expect(self.on, self.blk(turn(self.pos, 2), None))
@@ -197,7 +196,7 @@
 
     def wring(u, f):
         xx = turn(x, -u)
-        return Ring(z, at_z, lambda i, half: wblk(i, xx, f, half))
+        return Ring(z, at_z, wu.at[pl.ds(0, 256), pl.ds(0, 512)], lambda i, half: wblk(i, xx, f, half))
 
     wrings = {(u, f): wring(u, f) for u in range(4) for f in range(2)}
     a2a = {}
@@ -234,9 +233,9 @@
     for d in (1, 2, 3):
         pl.semaphore_signal(plane_x, inc=1, device_id=at_x(d), device_id_type=MESH)
         pl.semaphore_signal(plane_y, inc=1, device_id=at_y(d), device_id_type=MESH)
+    w_start(0, 0)
     pl.semaphore_wait(plane_x, 3)
     stat = exchange_start(sx_s, own_sums, sx_r, at_zx, 16)
-    w_start(0, 0)
     for d in (1, 3, 2):
         wu_send(d, 0)
     w_start(0, 1)
@@ -264,13 +263,14 @@
             col, size = col + part * 256, 256
         return nb.at[rows(yy * Q, Q, 32), rows(col, size, 256)]
 
-    a1 = Ring(x, at_x, lambda i, part: nblk(0, i, y, part))
-    b1 = Ring(y, at_y, lambda i, part: nblk(1, x, i, part))
+    two = nb.at[pl.ds(0, 2 * Q), pl.ds(0, 512)]
+    a1 = Ring(x, at_x, two, lambda i, part: nblk(0, i, y, part))
+    b1 = Ring(y, at_y, two, lambda i, part: nblk(1, x, i, part))
 
     def second(j):
         return (
-            Ring(y, at_y, lambda i, part: nblk(0, turn(x, -j), i, part)),
-            Ring(x, at_x, lambda i, part: nblk(1, i, turn(y, -j), part)),
+            Ring(y, at_y, two, lambda i, part: nblk(0, turn(x, -j), i, part)),
+            Ring(x, at_x, two, lambda i, part: nblk(1, i, turn(y, -j), part)),
         )
 
     seconds = [second(j) for j in range(4)]
@@ -480,7 +480,7 @@
                 return mob.at[i, place]
             return mob.at[i, place, pl.ds(half * 48, 48)]
 
-        ring = Ring(y, at_y, mblk)
+        ring = Ring(y, at_y, mob.at[pl.ds(0, 2), 0], mblk)
         ring.start()
         return ring
 
@@ -489,13 +489,13 @@
     fourth(0)
     gathers = [gather(places[0])]
     second_(1)
-    second_(2)
     h_finish(0)
     first(3)
+    second_(2)
+    h_finish(1)
+    first(4)
     third(1)
     gathers[0].forward()
-    h_finish(1)
-    first(4)
     third(2)
     third(3)
     fourth(1)
@@ -535,8 +535,8 @@
     pltpu.make_async_copy(obuf, out, local_sem.at[4]).wait()
 
 
-N_SEND = 64
-N_RECV = 126
+N_SEND = 40
+N_RECV = 105
 N_LOCAL = 5
 
 

time: 99.9 us -> 98 us (0.981)
  Pallas kernels: 97.7 us -> 95.8 us
    pallas_call x1, Pallas kernels: 97.7 us -> 95.8 us  [per_device(): pl.pallas_call(kernel, out_shape=jax.ShapeDtypeStruct((4, 4, Q, W), BF),...]
where the time goes in v7:
time: 98 us; the launch traced here: 97.8 us
  Pallas kernels  95.8 us (98%)
  local copies, waits for them, and re-layouts  2.06 us (2%)
    pallas_call x1, Pallas kernels, per_device(): pl.pallas_call(kernel, out_shape=jax.ShapeDtypeStruct((4, 4, Q, W), BF),...  95.8 us
    unnamed x1, local copies, waits for them, and re-layouts  2.06 us

profile of v7, /device:TPU:0, one launch (start us, length us, event | category | flops | bytes accessed | tf_op | source)
XLA Modules:
  0.0 97.8 jit_solution(3651088076288069384)
XLA Ops:
  0.0 95.8 %shard_map.82 = bf16[4,4,96,256]{3,2,1,0:T(8,128)(2,1)} custom-call(bf16[4,4,96,256]{3,2,1,0:T(8,128)(2,1)} %bitcast.8, bf16[4,4,96,256]{3,2,1,0:T(8,128)(2,1)} %bitcast.9, f32[1,256]{1,0:T(1,128)} %bitcast.10, f32[1,256]{1,0:T(1,128)} %bitcast.11, bf16[256,4096]{1,0:T(8,128)(2,1)} %wu_in.1, bf16[4096,256]{1,0:T(8,128)(2,1)} %wd_in.1, f32[1,256]{1,0:T(1,128)} %bitcast.12, ...), custom_call_target="tpu_custom_call" | custom-call | tf_op jit(solution)/shard_map/pallas_call | solution.py:547
  95.8 2.1 %copy.10 = bf16[1536,256]{1,0:T(8,128)(2,1)} copy(bf16[1536,256]{1,0:T(8,128)(2,1)} %bitcast.7) | data formatting | bytes 1572864

commit v8 on v7

--- a/solution.py
+++ b/solution.py
@@ -498,9 +498,9 @@
     gathers[0].forward()
     third(2)
     third(3)
+    third(4)
     fourth(1)
     gathers.append(gather(places[1]))
-    third(4)
     fourth(2)
     gathers.append(gather(places[2]))
     fourth(3)
@@ -535,7 +535,7 @@
     pltpu.make_async_copy(obuf, out, local_sem.at[4]).wait()
 
 
-N_SEND = 40
+N_SEND = 48
 N_RECV = 105
 N_LOCAL = 5
 

time: 98 us -> 96.4 us (0.984)
  Pallas kernels: 95.8 us -> 94.1 us
    pallas_call x1, Pallas kernels: 95.8 us -> 94.1 us  [per_device(): pl.pallas_call(kernel, out_shape=jax.ShapeDtypeStruct((4, 4, Q, W), BF),...]
where the time goes in v8:
time: 96.4 us; the launch traced here: 96.2 us
  Pallas kernels  94.1 us (98%)
  local copies, waits for them, and re-layouts  2.06 us (2%)
    pallas_call x1, Pallas kernels, per_device(): pl.pallas_call(kernel, out_shape=jax.ShapeDtypeStruct((4, 4, Q, W), BF),...  94.1 us
    unnamed x1, local copies, waits for them, and re-layouts  2.06 us

profile of v8, /device:TPU:0, one launch (start us, length us, event | category | flops | bytes accessed | tf_op | source)
XLA Modules:
  0.0 96.2 jit_solution(8245774204174662771)
XLA Ops:
  0.0 94.1 %shard_map.82 = bf16[4,4,96,256]{3,2,1,0:T(8,128)(2,1)} custom-call(bf16[4,4,96,256]{3,2,1,0:T(8,128)(2,1)} %bitcast.8, bf16[4,4,96,256]{3,2,1,0:T(8,128)(2,1)} %bitcast.9, f32[1,256]{1,0:T(1,128)} %bitcast.10, f32[1,256]{1,0:T(1,128)} %bitcast.11, bf16[256,4096]{1,0:T(8,128)(2,1)} %wu_in.1, bf16[4096,256]{1,0:T(8,128)(2,1)} %wd_in.1, f32[1,256]{1,0:T(1,128)} %bitcast.12, ...), custom_call_target="tpu_custom_call" | custom-call | tf_op jit(solution)/shard_map/pallas_call | solution.py:547
  94.1 2.1 %copy.10 = bf16[1536,256]{1,0:T(8,128)(2,1)} copy(bf16[1536,256]{1,0:T(8,128)(2,1)} %bitcast.7) | data formatting | bytes 1572864
